TPU v7x, 32 devices: a whole 2x2x4 slice. The times are simulated.
32 devices in a mesh: ep: 8 (over z, y), tp: 4 (over x, core).
Axes of the slice: x: 2, y: 2, z: 4, core: 2. Of those that a mesh axis runs over, the one named last changes fastest.
Arguments:
- tokens: bfloat16 [1024, 2048], P('ep'), may hold values from -6 to 6
- cotangent: bfloat16 [1024, 2048], P('ep'), may hold values from -6 to 6
- routing: int32 [1024, 2], P('ep'), may hold values from 0 to 7, all different within a row; in each aligned block of 128 rows (0 to 127, 128 to 255, ...) at most 64 rows name the same one
- router_weight: bfloat16 [2048, 8], replicated, may hold values from -0.125 to 0.125
- gate_weight: bfloat16 [8, 2048, 512], P('ep', None, 'tp'), may hold values from -0.125 to 0.125
- up_weight: bfloat16 [8, 2048, 512], P('ep', None, 'tp'), may hold values from -0.125 to 0.125
- down_weight: bfloat16 [8, 512, 2048], P('ep', 'tp'), may hold values from -0.25 to 0.25
Outputs:
- grad_tokens: bfloat16 [1024, 2048], P('ep', 'tp')
- grad_gating: float32 [1024, 2], P('ep')
- grad_router: float32 [2048, 8], P('ep')
- grad_gate_weight: bfloat16 [8, 2048, 512], P('ep', None, 'tp')
- grad_up_weight: bfloat16 [8, 2048, 512], P('ep', None, 'tp')
- grad_down_weight: bfloat16 [8, 512, 2048], P('ep', 'tp')
- in_norms: float32 [8, 2, 2048], P('ep')
- down_norms: float32 [8, 512], P('ep', 'tp')
- router_norms: float32 [2048], P('ep')
Inputs may be any that keep to these rules, and one draw needn't show every extreme that they name: `routing`: each row names 2 different experts. Among the rows of one index of ep no expert is named by more than 64 rows, a bound that some block reaches in some of them.
All inputs are finite; a program needn't handle non-finite values.
Results may differ from a plain program's by a relative error of at most 0.014.
Values may be sent and summed in bfloat16 or wider, within the bound.
A program may use at most 64 MiB of HBM per device.

v0:
```python
import functools

import jax
import jax.numpy as jnp
from jax import lax
from jax.experimental import pallas as pl
from jax.experimental.pallas import tpu as pltpu
from jax.sharding import PartitionSpec as P


def silu_parts(pre_gate):
    sigmoid_gate = jax.nn.sigmoid(pre_gate)
    return (pre_gate * sigmoid_gate, sigmoid_gate * (1.0 + pre_gate * (1.0 - sigmoid_gate)))


def slot_layout(routing, experts_all, capacity):
    tok_count, top_count = routing.shape
    flat_expert = routing.reshape(-1)
    one_hot = (flat_expert[:, None] == jnp.arange(experts_all, dtype=jnp.int32)[None, :]).astype(
        jnp.int32
    )
    earlier = jnp.cumsum(one_hot, axis=0) - one_hot
    within = jnp.sum(earlier * one_hot, axis=1)
    position = flat_expert * capacity + within
    vacant = jnp.full((experts_all * capacity,), tok_count * top_count, jnp.int32)
    return (vacant.at[position].set(jnp.arange(tok_count * top_count, dtype=jnp.int32)), position)


def general(tokens, cotangent, routing, router_weight, gate_weight, up_weight, down_weight):
    tok_count, model_width = tokens.shape
    top_count = routing.shape[1]
    experts_all = router_weight.shape[1]
    expert_local = gate_weight.shape[0]
    ep_size = lax.axis_size("ep")
    tp_size = lax.axis_size("tp")
    tp_index = lax.axis_index("tp")
    slice_width = model_width // tp_size
    capacity = max(2, 2 * tok_count * top_count // experts_all)
    arrived = ep_size * capacity
    logits = jnp.dot(tokens, router_weight, preferred_element_type=jnp.float32)
    picked = (
        routing[:, :, None] == jnp.arange(experts_all, dtype=jnp.int32)[None, None, :]
    ).astype(jnp.float32)
    scores = jax.nn.sigmoid(jnp.einsum("tke,te->tk", picked, logits))
    score_sum = jnp.sum(scores, axis=1, keepdims=True)
    gating = scores / score_sum
    assignment, position = slot_layout(routing, experts_all, capacity)
    source_row = assignment // top_count
    padded_tokens = jnp.concatenate([tokens, jnp.zeros((1, model_width), tokens.dtype)], axis=0)
    padded_cotangent = jnp.concatenate(
        [cotangent, jnp.zeros((1, model_width), cotangent.dtype)], axis=0
    )
    padded_gating = jnp.concatenate([gating.reshape(-1), jnp.zeros((1,), jnp.float32)])
    sent_gating = padded_gating[assignment].reshape(experts_all, capacity)
    own_tokens = lax.dynamic_slice_in_dim(padded_tokens, tp_index * slice_width, slice_width, 1)
    own_cotangent = lax.dynamic_slice_in_dim(
        padded_cotangent, tp_index * slice_width, slice_width, 1
    )
    part_tokens, part_cotangent = (
        lax.all_to_all(
            own_tokens[source_row].reshape(experts_all, capacity, slice_width),
            "ep",
            split_axis=0,
            concat_axis=0,
            tiled=True,
        ),
        lax.all_to_all(
            own_cotangent[source_row].reshape(experts_all, capacity, slice_width),
            "ep",
            split_axis=0,
            concat_axis=0,
            tiled=True,
        ),
    )
    got_tokens, got_cotangent = (
        lax.all_gather(part_tokens, "tp", axis=2, tiled=True),
        lax.all_gather(part_cotangent, "tp", axis=2, tiled=True),
    )
    got_gating = lax.all_to_all(sent_gating, "ep", split_axis=0, concat_axis=0, tiled=True)

    def by_expert(values):
        shaped = values.reshape((ep_size, expert_local) + values.shape[1:])
        return jnp.moveaxis(shaped, 1, 0).reshape((expert_local, arrived) + values.shape[2:])

    def by_source(values):
        shaped = values.reshape((expert_local, ep_size, capacity) + values.shape[2:])
        return jnp.moveaxis(shaped, 1, 0).reshape(
            (ep_size * expert_local, capacity) + values.shape[2:]
        )

    rows_in = by_expert(got_tokens)
    cot_rows = by_expert(got_cotangent)
    slot_gating = by_expert(got_gating)[:, :, None]
    pre_gate = jnp.einsum("lrd,ldf->lrf", rows_in, gate_weight, preferred_element_type=jnp.float32)
    pre_up = jnp.einsum("lrd,ldf->lrf", rows_in, up_weight, preferred_element_type=jnp.float32)
    activated, silu_slope = silu_parts(pre_gate)
    hidden = (activated * pre_up).astype(jnp.bfloat16)
    back_raw = jnp.einsum("lrd,lfd->lrf", cot_rows, down_weight, preferred_element_type=jnp.float32)
    hidden_wide = hidden.astype(jnp.float32)
    gate_partial = jnp.sum(hidden_wide * back_raw, axis=2)
    scaled_back = slot_gating * back_raw
    grad_pre_gate = (scaled_back * pre_up * silu_slope).astype(jnp.bfloat16)
    grad_pre_up = (scaled_back * activated).astype(jnp.bfloat16)
    scaled_hidden = (slot_gating * hidden_wide).astype(jnp.bfloat16)
    gate_sum = jnp.einsum(
        "lrd,lrf->ldf", rows_in, grad_pre_gate, preferred_element_type=jnp.float32
    )
    up_sum = jnp.einsum("lrd,lrf->ldf", rows_in, grad_pre_up, preferred_element_type=jnp.float32)
    down_sum = jnp.einsum(
        "lrf,lrd->lfd", scaled_hidden, cot_rows, preferred_element_type=jnp.float32
    )
    down_norms = jnp.sum(down_sum * down_sum, axis=2)
    back_partial = jnp.einsum(
        "lrf,ldf->lrd", grad_pre_gate, gate_weight, preferred_element_type=jnp.float32
    ) + jnp.einsum("lrf,ldf->lrd", grad_pre_up, up_weight, preferred_element_type=jnp.float32)
    back_rounded = back_partial.astype(jnp.bfloat16)
    slot_values = (
        lax.psum_scatter(back_rounded, "tp", scatter_dimension=2, tiled=True)
        .astype(jnp.float32)
        .astype(jnp.bfloat16)
    )
    gating_total, gate_rows, up_rows = lax.psum(
        (gate_partial, jnp.sum(gate_sum * gate_sum, axis=2), jnp.sum(up_sum * up_sum, axis=2)), "tp"
    )
    home_values = lax.all_to_all(
        by_source(slot_values), "ep", split_axis=0, concat_axis=0, tiled=True
    )
    home_gating = lax.all_to_all(
        by_source(gating_total), "ep", split_axis=0, concat_axis=0, tiled=True
    )
    flat_values = home_values.reshape(experts_all * capacity, slice_width)
    token_terms = (
        flat_values[position].reshape(tok_count, top_count, slice_width).astype(jnp.float32)
    )
    grad_gating = home_gating.reshape(-1)[position].reshape(tok_count, top_count)
    weighted = jnp.sum(gating * grad_gating, axis=1, keepdims=True)
    grad_scores = (grad_gating - weighted) / score_sum
    grad_chosen = grad_scores * scores * (1.0 - scores)
    grad_logits = jnp.einsum("tk,tke->te", grad_chosen, picked).astype(jnp.bfloat16)
    router_slice = lax.dynamic_slice_in_dim(router_weight, tp_index * slice_width, slice_width, 0)
    router_term = jnp.einsum(
        "te,de->td", grad_logits, router_slice, preferred_element_type=jnp.float32
    )
    grad_tokens = (jnp.sum(token_terms, axis=1) + router_term).astype(jnp.bfloat16)
    grad_router = lax.psum_scatter(
        jnp.einsum("td,te->de", tokens, grad_logits, preferred_element_type=jnp.float32),
        "ep",
        scatter_dimension=0,
        tiled=True,
    )
    router_norms = jnp.sum(grad_router * grad_router, axis=1)
    in_norms = jnp.stack([gate_rows, up_rows], axis=1)
    return (
        grad_tokens,
        grad_gating,
        grad_router,
        gate_sum.astype(jnp.bfloat16),
        up_sum.astype(jnp.bfloat16),
        down_sum.astype(jnp.bfloat16),
        in_norms,
        down_norms,
        router_norms,
    )


MESH = pl.DeviceIdType.MESH
F32 = jnp.float32
BF16 = jnp.bfloat16


def contract(a, b, dims, precision=None):
    return lax.dot_general(
        a, b, ((dims[0], dims[1]), ((), ())), precision=precision, preferred_element_type=F32
    )


def flipped(index, mask, bits):
    out = index
    for bit in range(bits):
        if (mask >> bit) & 1:
            out = out + (1 << bit) * (1 - 2 * ((index // (1 << bit)) % 2))
    return out


def kernel(n_ep, n_tp, cap,
           tok_hbm, cot_hbm, rt, rw, wg, wu, wd_hbm,
           o_tok, o_gg, o_gr, o_gate, o_up, o_down, o_norm, o_dnorm, o_rnorm,
           tok, cot, wgu, wd, sel, raw, info, other_x, ysa, ysx, arr_a, gs, gr, part, pc, xs, xr,
           fin, home, gp, sh, ggb, ggc, ggx, ggh, nb, nc, nx, rp, rr, lsem, ssem, rsem):
    e = lax.axis_index("ep")
    p = lax.axis_index("tp")
    n_z = n_ep // 2
    z, y = e // 2, e % 2
    toks, width = tok.shape
    n_exp = rw.shape[0]
    fb = width // n_tp
    hid = wd.shape[0]
    two = 2 * cap
    pieces = [(arr_a, b, b * fb, fb) for b in range(n_tp)]
    p_core, p_x, p_both = (flipped(p, m, 2) for m in (1, 2, 3))
    started, local = [], []

    def ep_at(d, h=0):
        return ((z + d) % n_z) * 2 + (y + h) % 2

    def send(source, dest, ep=None, tp=None):
        i = len(started)
        copy = pltpu.make_async_remote_copy(
            src_ref=source, dst_ref=dest, send_sem=ssem.at[i], recv_sem=rsem.at[i],
            device_id=(e if ep is None else ep, p if tp is None else tp), device_id_type=MESH)
        copy.start()
        started.append(copy)
        return copy

    def load(source, dest):
        copy = pltpu.make_async_copy(source, dest, lsem.at[len(local)])
        copy.start()
        local.append(copy)
        return copy

    barrier = pltpu.get_barrier_semaphore()
    offsets = [(0, 1)] + [(d, h) for d in (2, 1, 3) for h in (0, 1)]
    for d, h in offsets:
        pl.semaphore_signal(barrier, inc=1, device_id=(ep_at(d, h), p), device_id_type=MESH)
    for other in (p_core, p_x):
        pl.semaphore_signal(barrier, inc=1, device_id=(e, other), device_id_type=MESH)
    cols = pl.ds(pl.multiple_of(p * fb, 128), fb)
    cols_x = pl.ds(pl.multiple_of(p_x * fb, 128), fb)
    raw_in = [load(tok_hbm.at[:, cols], raw.at[0, 0]), load(cot_hbm.at[:, cols], raw.at[0, 1])]
    raw_in += [load(tok_hbm.at[:, cols_x], other_x.at[0]), load(cot_hbm.at[:, cols_x], other_x.at[1])]
    full_in = [load(tok_hbm, tok), load(cot_hbm, cot)]
    weights_in = [load(wg, wgu.at[:, pl.ds(0, hid)]), load(wu, wgu.at[:, pl.ds(hid, hid)]),
                  load(wd_hbm, wd)]

    r0, r1 = rt[0:1, :], rt[1:2, :]
    row_e = lax.broadcasted_iota(jnp.int32, (128, toks), 0)
    member_t = (r0 == row_e) | (r1 == row_e)
    earlier = (lax.broadcasted_iota(jnp.int32, (toks, toks), 0)
               < lax.broadcasted_iota(jnp.int32, (toks, toks), 1))
    place_t = contract(member_t.astype(F32).astype(BF16), earlier.astype(F32).astype(BF16),
                       ((1,), (0,)))
    place_t = jnp.where(member_t, place_t, -1000.0)
    info[0] = place_t[:n_exp]
    slot_id = lax.broadcasted_iota(jnp.int32, (cap, toks), 0).astype(F32)
    e_y = ep_at(0, 1)

    def chosen(d, x):
        return (info[d, pl.ds(x, 1), :] == slot_id).astype(F32).astype(BF16)

    for copy in raw_in:
        copy.wait()
    pl.semaphore_wait(barrier, n_ep + 1)

    right, left = ep_at(1), ep_at(n_z - 1)
    ring, infos = {}, {}
    for d in (1, 3, 2):
        infos[n_z - d] = send(info.at[0], info.at[n_z - d], ep=ep_at(d))
    for a in (0, 1):
        ring[3, a] = send(raw.at[0, a], raw.at[3, a], ep=right)
    for a in (0, 1):
        ring[1, a] = send(raw.at[0, a], raw.at[1, a], ep=left)

    to_y, xed, cored, cored2 = {}, {}, {}, {}

    def spread(src, a, key):
        xed[key, a] = send(arr_a.at[p, src, a], arr_a.at[p, src, a], tp=p_x)

    def pick(d, a):
        src = ep_at(d)
        if d:
            picks = jnp.concatenate([chosen(d, e_y), chosen(d, e)], axis=0)
        else:
            picks = chosen(d, e_y)
            ysx[a] = contract(picks, other_x[a], ((1,), (0,))).astype(BF16)
        rows = contract(picks, raw[d, a], ((1,), (0,))).astype(BF16)
        ysa[d, a] = rows[:cap]
        to_y[d, a] = [send(ysa.at[d, a], arr_a.at[p, src, a], ep=e_y)]
        if d:
            arr_a[p, src, a] = rows[cap:]
            spread(src, a, (d, 0))
        else:
            to_y[d, a].append(send(ysx.at[a], arr_a.at[p_x, src, a], ep=e_y))

    def arrive(d, a):
        ring[d, a].wait_recv()
        if d == 3:
            ring[2, a] = send(raw.at[3, a], raw.at[2, a], ep=right)
        pick(d, a)

    def from_y(d, a):
        for copy in to_y[d, a]:
            copy.wait_recv()
        if d:
            spread(ep_at(d, 1), a, (d, 1))

    def to_core(d, h):
        src = ep_at(d, h)
        cored[d, h] = send(arr_a.at[p, src], arr_a.at[p, src], tp=p_core)

    def x_to_core(d, h):
        if d:
            xed[(d, h), 0].wait_recv()
            xed[(d, h), 1].wait_recv()
        src = ep_at(d, h)
        cored2[d, h] = send(arr_a.at[p_x, src], arr_a.at[p_x, src], tp=p_core)

    pick(0, 0)
    pick(0, 1)

    for copy in full_in:
        copy.wait()
    for x in range(n_exp):
        sel[x] = (place_t[x:x + 1, :] == slot_id).astype(F32).astype(BF16)
    all_sel = sel[...].reshape(n_exp * cap, toks)
    place = jnp.transpose(place_t)
    member8 = place[:, :n_exp] > -1.0
    logits = contract(tok[...], rw[...], ((1,), (1,)))
    score = jnp.where(member8, jax.nn.sigmoid(logits), 0.0)
    score_sum = jnp.sum(score, axis=1, keepdims=True)
    gating = score / score_sum
    lane_s = (lax.broadcasted_iota(jnp.int32, (toks, two), 1) - y * cap).astype(F32)

    def hit(x):
        return (place[:, x:x + 1] == lane_s).astype(F32)

    for x in range(n_exp):
        row = jnp.sum(hit(x) * gating[:, x:x + 1], axis=0, keepdims=True)
        gs[x] = jnp.broadcast_to(row, (8, two))
    gated = {}
    for d, h in offsets:
        other = ep_at(d, h)
        gated[(n_z - d) % n_z, h] = send(gs.at[other], gr.at[e], ep=other)
    gr[e] = gs[e]
    own = sel[e]
    for a, ref in enumerate((tok, cot)):
        rows = contract(own, ref[...], ((1,), (0,))).astype(BF16)
        for ref_b, b, start, size in pieces:
            ref_b[b, e, a] = rows[:, start:start + size]

    ret_c, ret_x, ret_f = {}, {}, {}

    def base_of(q):
        return ((z + q) % n_z) * 2

    def compute(q):
        for h in ((1,) if q == 0 else (0, 1)):
            gated[q, h].wait_recv()
            cored[q, h].wait_recv()
            cored2[q, h].wait_recv()
        base = base_of(q)
        pair = pl.ds(base, 2)
        here = pl.ds(pl.multiple_of(base * cap, two), two)
        pre = jnp.zeros((two, 2 * hid), F32)
        back = jnp.zeros((two, hid), F32)
        for ref_b, b, start, size in pieces:
            c = slice(start, start + size)
            pre = pre + contract(ref_b[b, pair, 0].reshape(two, size), wgu[c, :], ((1,), (0,)))
            back = back + contract(ref_b[b, pair, 1].reshape(two, size), wd[:, c], ((1,), (1,)))
        gate = jnp.transpose(gr[base] + gr[base + 1])[:, 0:1]
        pre_gate, pre_up = pre[:, :hid], pre[:, hid:]
        activated, slope = silu_parts(pre_gate)
        hidden = (activated * pre_up).astype(BF16).astype(F32)
        prod = hidden * back
        ggb[base // 2] = contract(jnp.ones((8, hid), F32), prod, ((1,), (1,)),
                                  lax.Precision.HIGHEST)
        scaled = gate * back
        grads = jnp.concatenate([(scaled * pre_up * slope).astype(BF16),
                                 (scaled * activated).astype(BF16)], axis=1)
        gp[here, :] = grads
        sh[here, :] = (gate * hidden).astype(BF16)
        for b in range(n_tp):
            part[b, pair] = contract(grads, wgu[b * fb:(b + 1) * fb, :], ((1,), (1,))).astype(
                BF16).reshape(2, cap, fb)
        ret_c[q] = (send(part.at[p_both, pair], pc.at[1, pair], tp=p_core),
                    send(part.at[p_core, pair], pc.at[0, pair], tp=p_core))

    def to_x(q):
        pair = pl.ds(base_of(q), 2)
        ret_c[q][0].wait_recv()
        xs[pair] = (part[p_x, pair].astype(F32) + pc[1, pair].astype(F32)).astype(BF16)
        ret_x[q] = send(xs.at[pair], xr.at[pair], tp=p_x)

    def to_home(q):
        pair = pl.ds(base_of(q), 2)
        ret_c[q][1].wait_recv()
        ret_x[q].wait_recv()
        fin[pair] = (part[p, pair].astype(F32) + pc[0, pair].astype(F32)
                     + xr[pair].astype(F32)).astype(BF16)
        for h in ((1,) if q == 0 else (0, 1)):
            other = ep_at(q, h)
            ret_f[q, h] = send(fin.at[other], home.at[e], ep=other)
        if q == 0:
            home[e] = fin[e]

    for d in (3, 1, 2):
        infos[d].wait_recv()
    from_y(0, 0)
    from_y(0, 1)
    to_core(0, 1)
    x_to_core(0, 1)
    arrive(3, 0)
    from_y(3, 0)
    arrive(3, 1)
    to_core(3, 0)
    from_y(3, 1)
    to_core(3, 1)
    for copy in weights_in:
        copy.wait()
    compute(0)
    arrive(1, 0)
    x_to_core(3, 0)
    from_y(1, 0)
    to_x(0)
    arrive(1, 1)
    to_core(1, 0)
    x_to_core(3, 1)
    from_y(1, 1)
    to_core(1, 1)
    compute(3)
    to_home(0)
    arrive(2, 0)
    from_y(2, 0)
    x_to_core(1, 0)
    to_x(3)
    arrive(2, 1)
    to_core(2, 0)
    x_to_core(1, 1)
    from_y(2, 1)
    to_core(2, 1)
    compute(1)
    to_home(3)
    x_to_core(2, 0)
    x_to_core(2, 1)
    to_x(1)
    compute(2)
    last = 2
    gg_c = send(ggb, ggc, tp=p_core)
    to_x(last)
    gg_c.wait_recv()
    ggb2 = ggb[...] + ggc[...]
    ggc[...] = ggb2
    gg_x = send(ggc, ggx, tp=p_x)
    to_home(1)
    grads = gp[...]

    def in_block(i):
        ref_b, b, start, size = pieces[i]
        rows = ref_b[b, :, 0].reshape(n_ep * cap, size)
        sums = contract(grads, rows, ((0,), (0,)))
        c = slice(start, start + size)
        o_gate[c, :] = jnp.transpose(sums[:hid]).astype(BF16)
        o_up[c, :] = jnp.transpose(sums[hid:]).astype(BF16)
        nb[0:1, c] = jnp.sum(sums[:hid] * sums[:hid], axis=0, keepdims=True)
        nb[1:2, c] = jnp.sum(sums[hid:] * sums[hid:], axis=0, keepdims=True)

    in_block(0)
    gg_x.wait_recv()
    ggx[...] = ggb2 + ggx[...]
    gg_f = {}
    for k in offsets:
        other = ep_at(*k)
        gg_f[k] = send(ggx.at[other // 2], ggh.at[e], ep=other)
    ggh[e] = ggx[e // 2]
    in_block(1)
    to_home(last)
    for i in range(2, len(pieces)):
        in_block(i)
    nb_c = send(nb, nc, tp=p_core)

    for k in offsets:
        gg_f[k].wait_recv()
    lane8 = lax.broadcasted_iota(jnp.int32, (toks, n_exp), 1)
    got = jnp.zeros((toks, n_exp), F32)
    for x in range(n_exp):
        col = jnp.sum(hit(x) * ggh[x, 0:1, :], axis=1, keepdims=True)
        got = got + jnp.where(lane8 == x, col, 0.0)
    got_t = jnp.transpose(jnp.concatenate(
        [got, jnp.zeros((toks, 128 - n_exp), F32)], axis=1))[:n_exp]
    for k, r in enumerate((r0, r1)):
        o_gg[k:k + 1, :] = jnp.sum(jnp.where(r == row_e[:n_exp], got_t, 0.0), axis=0, keepdims=True)
    weighted = jnp.sum(gating * got, axis=1, keepdims=True)
    grad_logits = jnp.where(member8, (got - weighted) / score_sum * score * (1.0 - score),
                            0.0).astype(BF16)
    rp[...] = contract(grad_logits, tok[...], ((0,), (0,)))
    span = width // n_ep
    rr_f = {}
    for k in offsets:
        other = ep_at(*k)
        rr_f[k] = send(rp.at[:, pl.ds(pl.multiple_of(other * span, 128), span)], rr.at[e], ep=other)
    rr[e] = rp[:, pl.ds(pl.multiple_of(e * span, 128), span)]
    nb_c.wait_recv()
    nc[...] = nb[...] + nc[...]
    nb_x = send(nc, nx, tp=p_x)
    shv = sh[...]
    dn = jnp.zeros((hid, 1), F32)
    for ref_b, b, start, size in pieces:
        sums = contract(shv, ref_b[b, :, 1].reshape(n_ep * cap, size), ((0,), (0,)))
        o_down[:, start:start + size] = sums.astype(BF16)
        dn = dn + jnp.sum(sums * sums, axis=1, keepdims=True)
    o_dnorm[...] = jnp.transpose(jnp.broadcast_to(dn, (hid, 128)))[0:1, :]
    router_term = contract(grad_logits, rw[:, cols], ((1,), (0,)))
    nb_x.wait_recv()
    o_norm[...] = nc[...] + nx[...]
    for k in offsets:
        rr_f[k].wait_recv()
    total = rr[0]
    for x in range(1, n_ep):
        total = total + rr[x]
    o_gr[...] = total
    o_rnorm[...] = jnp.sum(total * total, axis=0, keepdims=True)
    for k in offsets:
        ret_f[k].wait_recv()
    o_tok[...] = (contract(all_sel, home[...].reshape(n_exp * cap, fb), ((0,), (0,)))
                  + router_term).astype(BF16)
    for copy in started:
        copy.wait_send()


def fused(tokens, cotangent, routing, router_weight, gate_weight, up_weight, down_weight):
    n_ep, n_tp = lax.axis_size("ep"), lax.axis_size("tp")
    toks, width = tokens.shape
    n_exp = router_weight.shape[1]
    cap = max(2, 2 * toks * routing.shape[1] // n_exp)
    hid = gate_weight.shape[2]
    fb = width // n_tp
    two = 2 * cap
    slots = n_ep * cap
    span = width // n_ep
    copies = 16 * n_ep
    vmem = pl.BlockSpec(memory_space=pltpu.VMEM)
    hbm = pl.BlockSpec(memory_space=pltpu.HBM)
    outs = pl.pallas_call(
        functools.partial(kernel, n_ep, n_tp, cap),
        out_shape=[
            jax.ShapeDtypeStruct((toks, fb), BF16),
            jax.ShapeDtypeStruct((routing.shape[1], toks), F32),
            jax.ShapeDtypeStruct((n_exp, span), F32),
            jax.ShapeDtypeStruct((width, hid), BF16),
            jax.ShapeDtypeStruct((width, hid), BF16),
            jax.ShapeDtypeStruct((hid, width), BF16),
            jax.ShapeDtypeStruct((2, width), F32),
            jax.ShapeDtypeStruct((1, hid), F32),
            jax.ShapeDtypeStruct((1, span), F32),
        ],
        in_specs=[hbm] * 2 + [vmem] * 2 + [hbm] * 3,
        out_specs=[vmem] * 9,
        scratch_shapes=[
            pltpu.VMEM((toks, width), BF16),
            pltpu.VMEM((toks, width), BF16),
            pltpu.VMEM((width, 2 * hid), BF16),
            pltpu.VMEM((hid, width), BF16),
            pltpu.VMEM((n_exp, cap, toks), BF16),
            pltpu.VMEM((n_ep // 2, 2, toks, fb), BF16),
            pltpu.VMEM((n_ep // 2, n_exp, toks), F32),
            pltpu.VMEM((2, toks, fb), BF16),
            pltpu.VMEM((n_ep // 2, 2, cap, fb), BF16),
            pltpu.VMEM((2, cap, fb), BF16),
            pltpu.VMEM((n_tp, n_ep, 2, cap, fb), BF16),
            pltpu.VMEM((n_exp, 8, two), F32),
            pltpu.VMEM((n_ep, 8, two), F32),
            pltpu.VMEM((n_tp, n_ep, cap, fb), BF16),
            pltpu.VMEM((2, n_ep, cap, fb), BF16),
            pltpu.VMEM((n_ep, cap, fb), BF16),
            pltpu.VMEM((n_ep, cap, fb), BF16),
            pltpu.VMEM((n_ep, cap, fb), BF16),
            pltpu.VMEM((n_exp, cap, fb), BF16),
            pltpu.VMEM((slots, 2 * hid), BF16),
            pltpu.VMEM((slots, hid), BF16),
            pltpu.VMEM((n_ep // 2, 8, two), F32),
            pltpu.VMEM((n_ep // 2, 8, two), F32),
            pltpu.VMEM((n_ep // 2, 8, two), F32),
            pltpu.VMEM((n_exp, 8, two), F32),
            pltpu.VMEM((2, width), F32),
            pltpu.VMEM((2, width), F32),
            pltpu.VMEM((2, width), F32),
            pltpu.VMEM((n_exp, width), F32),
            pltpu.VMEM((n_ep, n_exp, span), F32),
            pltpu.SemaphoreType.DMA((9,)),
            pltpu.SemaphoreType.DMA((copies,)),
            pltpu.SemaphoreType.DMA((copies,)),
        ],
        compiler_params=pltpu.CompilerParams(
            collective_id=0, has_side_effects=True, vmem_limit_bytes=67043328
        ),
    )(tokens, cotangent, routing.T, router_weight.T, gate_weight[0], up_weight[0], down_weight[0])
    o_tok, o_gg, o_gr, o_gate, o_up, o_down, o_norm, o_dnorm, o_rnorm = outs
    return (o_tok, o_gg.T, o_gr.T, o_gate[None], o_up[None], o_down[None], o_norm[None],
            o_dnorm, o_rnorm[0])


def shards(tokens, cotangent, routing, router_weight, gate_weight, up_weight, down_weight):
    n_ep, n_tp = lax.axis_size("ep"), lax.axis_size("tp")
    toks, width = tokens.shape
    n_exp = router_weight.shape[1]
    cap = max(2, 2 * toks * routing.shape[1] // n_exp)
    fits = (
        n_tp == 4 and n_ep == 8 and n_ep == n_exp
        and 2 * cap == toks == 128 and gate_weight.shape[2] == 128
        and routing.shape[1] == 2 and width % (128 * 8) == 0
    )
    form = fused if fits else general
    return form(tokens, cotangent, routing, router_weight, gate_weight, up_weight, down_weight)


def solution(mesh):
    in_specs = (
        P("ep", None),
        P("ep", None),
        P("ep", None),
        P(),
        P("ep", None, "tp"),
        P("ep", None, "tp"),
        P("ep", "tp", None),
    )
    out_specs = (
        P("ep", "tp"),
        P("ep", None),
        P("ep", None),
        P("ep", None, "tp"),
        P("ep", None, "tp"),
        P("ep", "tp", None),
        P("ep", None, None),
        P("ep", "tp"),
        P("ep"),
    )
    return jax.shard_map(shards, mesh=mesh, in_specs=in_specs, out_specs=out_specs, check_vma=False)
```

profile of v0, /device:TPU:0, one launch (start us, length us, event | category | flops | bytes accessed | tf_op | source)
XLA Modules:
  0.0 72.0 jit_solution(3581096955639420086)
XLA Ops:
  0.6 62.7 %shard_map.142 = (bf16[128,512]{1,0:T(8,128)(2,1)}, f32[2,128]{1,0:T(2,128)}, f32[8,256]{1,0:T(8,128)}, bf16[2048,128]{1,0:T(8,128)(2,1)}, bf16[2048,128]{1,0:T(...) custom-call(bf16[128,2048]{1,0:T(8,128)(2,1)} %tok_hbm.1, ...), custom_call_target="tpu_custom_call" | custom-call | tf_op jit(solution)/shard_map/pallas_call | solution.py:532
  63.3 0.0 copy-start.5
  63.4 0.0 copy-start.3
  63.4 1.6 %copy.25 = bf16[128,512]{1,0:T(8,128)(2,1)} copy(bf16[128,512]{1,0:T(8,128)(2,1)} %get-tuple-element.36) | data formatting | bytes 262144
  64.9 0.0 copy-done.5
  64.9 0.6 copy.26
  65.5 0.0 copy-done.3
  65.5 0.6 copy.27
  66.1 0.0 copy-start.1
  66.1 1.9 %copy.28 = bf16[1,2048,128]{2,1,0:T(8,128)(2,1)} copy(bf16[1,2048,128]{2,1,0:T(8,128)(2,1)} %bitcast.17) | data formatting | bytes 1048576
  68.0 0.0 copy-done.1
  68.0 0.0 copy-start
  68.0 0.8 %copy.29 = bf16[1,2048,128]{2,1,0:T(8,128)(2,1)} copy(bf16[1,2048,128]{2,1,0:T(8,128)(2,1)S(1)} %bitcast.16) | data formatting | bytes 1048576
  68.8 0.4 copy-done
  69.3 0.0 copy-start.2
  69.3 0.8 %copy.30 = bf16[1,128,2048]{2,1,0:T(8,128)(2,1)} copy(bf16[1,128,2048]{2,1,0:T(8,128)(2,1)S(1)} %bitcast.15) | data formatting | bytes 1048576
  70.1 0.0 copy-done.2
  70.1 0.0 copy-start.6
  70.1 0.6 copy.31
  70.7 0.1 copy-done.6
  70.7 0.0 copy-start.4
  70.7 0.5 copy.32
  71.2 0.1 copy-done.4
  71.4 0.6 copy.33
Async XLA Ops:
  63.3 1.6 %copy-start.5 = (f32[2,128]{1,0:T(2,128)S(1)}, f32[2,128]{1,0:T(2,128)}, u32[]{:S(2)}) copy-start(f32[2,128]{1,0:T(2,128)} %get-tuple-element.19) | copy-start | bytes 3076
  63.4 2.2 %copy-start.3 = (f32[8,256]{1,0:T(8,128)S(1)}, f32[8,256]{1,0:T(8,128)}, u32[]{:S(2)}) copy-start(f32[8,256]{1,0:T(8,128)} %get-tuple-element.20) | copy-start | bytes 24580
  66.1 1.9 %copy-start.1 = (bf16[2048,128]{1,0:T(8,128)(2,1)S(1)}, bf16[2048,128]{1,0:T(8,128)(2,1)}, u32[]{:S(2)}) copy-start(bf16[2048,128]{1,0:T(8,128)(2,1)} %get-tuple-element.22) | copy-start | bytes 1572868
  68.0 1.2 %copy-start = (bf16[128,2048]{1,0:T(8,128)(2,1)S(1)}, bf16[128,2048]{1,0:T(8,128)(2,1)}, u32[]{:S(2)}) copy-start(bf16[128,2048]{1,0:T(8,128)(2,1)} %get-tuple-element.23) | copy-start | bytes 1572868
  69.3 0.8 %copy-start.2 = (f32[2,2048]{1,0:T(2,128)S(1)}, f32[2,2048]{1,0:T(2,128)}, u32[]{:S(2)}) copy-start(f32[2,2048]{1,0:T(2,128)} %get-tuple-element.24) | copy-start | bytes 49156
  70.1 0.7 copy-start.6
  70.7 0.7 copy-start.4
where the time goes:
time: 72.3 us; the launch traced here: 72 us
  Pallas kernels  62.7 us (87%)
  local copies, waits for them, and re-layouts  8.58 us (12%)
    pallas_call x1, Pallas kernels, fused(): pl.pallas_call(functools.partial(kernel, n_ep, n_tp, cap), out_shape=[jax...  62.7 us
    unnamed x23, local copies, waits for them, and re-layouts  8.58 us

commit v1 on v0

--- a/solution.py
+++ b/solution.py
@@ -183,9 +183,9 @@
 
 
 def kernel(n_ep, n_tp, cap,
-           tok_hbm, cot_hbm, rt, rw, wg, wu, wd_hbm,
+           tok_hbm, cot_hbm, rt_hbm, rw_hbm, wg, wu, wd_hbm,
            o_tok, o_gg, o_gr, o_gate, o_up, o_down, o_norm, o_dnorm, o_rnorm,
-           tok, cot, wgu, wd, sel, raw, info, other_x, ysa, ysx, arr_a, gs, gr, part, pc, xs, xr,
+           rt, rw, tok, cot, wgu, wd, sel, raw, info, other_x, ysa, ysx, arr_a, gs, gr, part, pc, xs, xr,
            fin, home, gp, sh, ggb, ggc, ggx, ggh, nb, nc, nx, rp, rr, lsem, ssem, rsem):
     e = lax.axis_index("ep")
     p = lax.axis_index("tp")
@@ -224,14 +224,16 @@
         pl.semaphore_signal(barrier, inc=1, device_id=(ep_at(d, h), p), device_id_type=MESH)
     for other in (p_core, p_x):
         pl.semaphore_signal(barrier, inc=1, device_id=(e, other), device_id_type=MESH)
+    routing_in = load(rt_hbm, rt)
     cols = pl.ds(pl.multiple_of(p * fb, 128), fb)
     cols_x = pl.ds(pl.multiple_of(p_x * fb, 128), fb)
     raw_in = [load(tok_hbm.at[:, cols], raw.at[0, 0]), load(cot_hbm.at[:, cols], raw.at[0, 1])]
     raw_in += [load(tok_hbm.at[:, cols_x], other_x.at[0]), load(cot_hbm.at[:, cols_x], other_x.at[1])]
-    full_in = [load(tok_hbm, tok), load(cot_hbm, cot)]
+    full_in = [load(rw_hbm, rw), load(tok_hbm, tok), load(cot_hbm, cot)]
     weights_in = [load(wg, wgu.at[:, pl.ds(0, hid)]), load(wu, wgu.at[:, pl.ds(hid, hid)]),
                   load(wd_hbm, wd)]
 
+    routing_in.wait()
     r0, r1 = rt[0:1, :], rt[1:2, :]
     row_e = lax.broadcasted_iota(jnp.int32, (128, toks), 0)
     member_t = (r0 == row_e) | (r1 == row_e)
@@ -516,6 +518,15 @@
         copy.wait_send()
 
 
+def flush(*refs):
+    sem = refs[-1]
+    copies = [pltpu.make_async_copy(refs[i], refs[9 + i], sem.at[i]) for i in range(9)]
+    for copy in copies:
+        copy.start()
+    for copy in copies:
+        copy.wait()
+
+
 def fused(tokens, cotangent, routing, router_weight, gate_weight, up_weight, down_weight):
     n_ep, n_tp = lax.axis_size("ep"), lax.axis_size("tp")
     toks, width = tokens.shape
@@ -527,24 +538,27 @@
     slots = n_ep * cap
     span = width // n_ep
     copies = 16 * n_ep
+    results = [
+        ((toks, fb), BF16),
+        ((routing.shape[1], toks), F32),
+        ((n_exp, span), F32),
+        ((width, hid), BF16),
+        ((width, hid), BF16),
+        ((hid, width), BF16),
+        ((2, width), F32),
+        ((1, hid), F32),
+        ((1, span), F32),
+    ]
     vmem = pl.BlockSpec(memory_space=pltpu.VMEM)
     hbm = pl.BlockSpec(memory_space=pltpu.HBM)
     outs = pl.pallas_call(
         functools.partial(kernel, n_ep, n_tp, cap),
-        out_shape=[
-            jax.ShapeDtypeStruct((toks, fb), BF16),
-            jax.ShapeDtypeStruct((routing.shape[1], toks), F32),
-            jax.ShapeDtypeStruct((n_exp, span), F32),
-            jax.ShapeDtypeStruct((width, hid), BF16),
-            jax.ShapeDtypeStruct((width, hid), BF16),
-            jax.ShapeDtypeStruct((hid, width), BF16),
-            jax.ShapeDtypeStruct((2, width), F32),
-            jax.ShapeDtypeStruct((1, hid), F32),
-            jax.ShapeDtypeStruct((1, span), F32),
-        ],
-        in_specs=[hbm] * 2 + [vmem] * 2 + [hbm] * 3,
+        out_shape=[pltpu.VMEM(shape, dtype) for shape, dtype in results],
+        in_specs=[hbm] * 7,
         out_specs=[vmem] * 9,
         scratch_shapes=[
+            pltpu.VMEM((routing.shape[1], toks), jnp.int32),
+            pltpu.VMEM((n_exp, width), BF16),
             pltpu.VMEM((toks, width), BF16),
             pltpu.VMEM((toks, width), BF16),
             pltpu.VMEM((width, 2 * hid), BF16),
@@ -575,14 +589,23 @@
             pltpu.VMEM((2, width), F32),
             pltpu.VMEM((n_exp, width), F32),
             pltpu.VMEM((n_ep, n_exp, span), F32),
-            pltpu.SemaphoreType.DMA((9,)),
+            pltpu.SemaphoreType.DMA((11,)),
             pltpu.SemaphoreType.DMA((copies,)),
             pltpu.SemaphoreType.DMA((copies,)),
         ],
         compiler_params=pltpu.CompilerParams(
-            collective_id=0, has_side_effects=True, vmem_limit_bytes=67043328
+            collective_id=0, has_side_effects=True, vmem_limit_bytes=40 << 20
         ),
-    )(tokens, cotangent, routing.T, router_weight.T, gate_weight[0], up_weight[0], down_weight[0])
+    )(*[pltpu.with_memory_space_constraint(v, pltpu.HBM)
+        for v in (tokens, cotangent, routing.T, router_weight.T,
+                  gate_weight[0], up_weight[0], down_weight[0])])
+    outs = pl.pallas_call(
+        flush,
+        out_shape=[jax.ShapeDtypeStruct(shape, dtype) for shape, dtype in results],
+        in_specs=[vmem] * 9,
+        out_specs=[hbm] * 9,
+        scratch_shapes=[pltpu.SemaphoreType.DMA((9,))],
+    )(*[pltpu.with_memory_space_constraint(v, pltpu.VMEM) for v in outs])
     o_tok, o_gg, o_gr, o_gate, o_up, o_down, o_norm, o_dnorm, o_rnorm = outs
     return (o_tok, o_gg.T, o_gr.T, o_gate[None], o_up[None], o_down[None], o_norm[None],
             o_dnorm, o_rnorm[0])

time: 72.3 us -> 62.9 us (0.87)
  local copies, waits for them, and re-layouts: 8.58 us -> 0 us
    unnamed x23 -> x0, local copies, waits for them, and re-layouts: 8.58 us -> none
    pallas_call x1 -> x2, Pallas kernels: 62.7 us -> 62.1 us  [the longest x1 60.8 us: fused(): pl.pallas_call(functools.partial(kernel, n_ep, n_tp, cap), out_shape=[plt...]
where the time goes in v1:
time: 62.9 us; the launch traced here: 62.7 us
  Pallas kernels  62.1 us (99%)
  between operations  0.65 us (1%)
    pallas_call x1, Pallas kernels, fused(): pl.pallas_call(functools.partial(kernel, n_ep, n_tp, cap), out_shape=[plt...  60.8 us
    pallas_call x1, Pallas kernels, fused(): pl.pallas_call(flush, out_shape=[jax.ShapeDtypeStruct(shape, dtype) for s...  1.28 us

profile of v1, /device:TPU:0, one launch (start us, length us, event | category | flops | bytes accessed | tf_op | source)
XLA Modules:
  0.0 62.7 jit_solution(17481559926596976757)
XLA Ops:
  0.6 60.8 %shard_map.142 = (bf16[128,512]{1,0:T(8,128)(2,1)S(1)}, f32[2,128]{1,0:T(2,128)S(1)}, f32[8,256]{1,0:T(8,128)S(1)}, bf16[2048,128]{1,0:T(8,128)(2,1)S(1)}, bf16[...) custom-call(bf16[128,2048]{1,0:T(8,128)(2,1)} %tok_hbm.1, ...), custom_call_target="tpu_custom_call" | custom-call | tf_op jit(solution)/shard_map/pallas_call | solution.py:554
  61.4 1.3 %shard_map.143 = (bf16[128,512]{1,0:T(8,128)(2,1)}, f32[2,128]{1,0:T(2,128)}, f32[8,256]{1,0:T(8,128)}, bf16[2048,128]{1,0:T(8,128)(2,1)}, bf16[2048,128]{1,0:T(...) custom-call(bf16[128,512]{1,0:T(8,128)(2,1)S(1)} %get-tuple-element.27.refs_0_, ...), custom_call_target="tpu_custom_call" | custom-call | tf_op jit(solution)/shard_map/pallas_call | solution.py:602

commit v2 on v1

--- a/solution.py
+++ b/solution.py
@@ -1,4 +1,5 @@
 import functools
+import math
 
 import jax
 import jax.numpy as jnp
@@ -164,6 +165,7 @@
 
 
 MESH = pl.DeviceIdType.MESH
+RAW, TO_Y, TO_X, TO_CORE, BACK, HOME, SMALL = range(7)
 F32 = jnp.float32
 BF16 = jnp.bfloat16
 
@@ -185,32 +187,51 @@
 def kernel(n_ep, n_tp, cap,
            tok_hbm, cot_hbm, rt_hbm, rw_hbm, wg, wu, wd_hbm,
            o_tok, o_gg, o_gr, o_gate, o_up, o_down, o_norm, o_dnorm, o_rnorm,
-           rt, rw, tok, cot, wgu, wd, sel, raw, info, other_x, ysa, ysx, arr_a, gs, gr, part, pc, xs, xr,
-           fin, home, gp, sh, ggb, ggc, ggx, ggh, nb, nc, nx, rp, rr, lsem, ssem, rsem):
+           rt, rw, tok, cot, wgu, wd, sel, raw, info, other_x, raw_x, ysa, ysx, ysw, arr_a, gall, mid, part, pc, xs, xr,
+           fin, home, gp, sh, ggb, ggc, ggs, ggh, gts, nb, nc, nx, rp, rr, lsem, ssem, rsem):
     e = lax.axis_index("ep")
     p = lax.axis_index("tp")
-    n_z = n_ep // 2
     z, y = e // 2, e % 2
+    x_me = p // 2
     toks, width = tok.shape
     n_exp = rw.shape[0]
     fb = width // n_tp
     hid = wd.shape[0]
     two = 2 * cap
-    pieces = [(arr_a, b, b * fb, fb) for b in range(n_tp)]
     p_core, p_x, p_both = (flipped(p, m, 2) for m in (1, 2, 3))
-    started, local = [], []
-
-    def ep_at(d, h=0):
-        return ((z + d) % n_z) * 2 + (y + h) % 2
-
-    def send(source, dest, ep=None, tp=None):
-        i = len(started)
-        copy = pltpu.make_async_remote_copy(
-            src_ref=source, dst_ref=dest, send_sem=ssem.at[i], recv_sem=rsem.at[i],
+    z_pair, z_mid = flipped(z, 1, 1), 3 - z
+    is_mid = (z == 1) | (z == 2)
+    is_edge = jnp.logical_not(is_mid)
+    planes = (z, z_pair, 2 - z // 2, 3 - 3 * (z // 2))
+    e_y = z * 2 + 1 - y
+    sends, slots, local, branch = {}, {}, [], ["all"]
+
+    def ep_of(plane, h=0):
+        return plane * 2 + (y + h) % 2
+
+    def receiver(arrival):
+        return slots.setdefault(arrival, len(slots))
+
+    def transfer(group, arrival, source, dest, ep=None, tp=None):
+        return pltpu.make_async_remote_copy(
+            src_ref=source, dst_ref=dest, send_sem=ssem.at[group],
+            recv_sem=rsem.at[receiver(arrival)],
             device_id=(e if ep is None else ep, p if tp is None else tp), device_id_type=MESH)
-        copy.start()
-        started.append(copy)
-        return copy
+
+    def send(key, source, dest, group, ep=None, tp=None, arrival=None):
+        transfer(group, key if arrival is None else arrival, source, dest, ep, tp).start()
+        unit = n_exp * 128 if group == SMALL else cap * fb
+        sends[branch[-1], key] = (group, math.prod(source.shape) // unit)
+
+    def only(cond, name, body):
+        @pl.when(cond)
+        def _():
+            branch.append(name)
+            body()
+            branch.pop()
+
+    def landed(arrival, ref):
+        transfer(0, arrival, ref, ref).wait_recv()
 
     def load(source, dest):
         copy = pltpu.make_async_copy(source, dest, lsem.at[len(local)])
@@ -219,15 +240,18 @@
         return copy
 
     barrier = pltpu.get_barrier_semaphore()
-    offsets = [(0, 1)] + [(d, h) for d in (2, 1, 3) for h in (0, 1)]
-    for d, h in offsets:
-        pl.semaphore_signal(barrier, inc=1, device_id=(ep_at(d, h), p), device_id_type=MESH)
-    for other in (p_core, p_x):
-        pl.semaphore_signal(barrier, inc=1, device_id=(e, other), device_id_type=MESH)
+    pl.semaphore_signal(barrier, inc=1, device_id=(ep_of(z_pair), p), device_id_type=MESH)
+
+    @pl.when(is_mid)
+    def _():
+        pl.semaphore_signal(barrier, inc=1, device_id=(ep_of(z_mid), p), device_id_type=MESH)
+
+    for ep, tp in ((e_y, p_x), (e_y, p), (e, p_x), (e, p_core)):
+        pl.semaphore_signal(barrier, inc=1, device_id=(ep, tp), device_id_type=MESH)
     routing_in = load(rt_hbm, rt)
     cols = pl.ds(pl.multiple_of(p * fb, 128), fb)
     cols_x = pl.ds(pl.multiple_of(p_x * fb, 128), fb)
-    raw_in = [load(tok_hbm.at[:, cols], raw.at[0, 0]), load(cot_hbm.at[:, cols], raw.at[0, 1])]
+    raw_in = [load(tok_hbm.at[:, cols], raw.at[z, 0]), load(cot_hbm.at[:, cols], raw.at[z, 1])]
     raw_in += [load(tok_hbm.at[:, cols_x], other_x.at[0]), load(cot_hbm.at[:, cols_x], other_x.at[1])]
     full_in = [load(rw_hbm, rw), load(tok_hbm, tok), load(cot_hbm, cot)]
     weights_in = [load(wg, wgu.at[:, pl.ds(0, hid)]), load(wu, wgu.at[:, pl.ds(hid, hid)]),
@@ -241,281 +265,420 @@
                < lax.broadcasted_iota(jnp.int32, (toks, toks), 1))
     place_t = contract(member_t.astype(F32).astype(BF16), earlier.astype(F32).astype(BF16),
                        ((1,), (0,)))
-    place_t = jnp.where(member_t, place_t, -1000.0)
-    info[0] = place_t[:n_exp]
+    place_t = jnp.where(member_t, place_t, -1000.0)[:n_exp]
+    member_t = member_t[:n_exp]
+    info[z] = place_t
     slot_id = lax.broadcasted_iota(jnp.int32, (cap, toks), 0).astype(F32)
-    e_y = ep_at(0, 1)
-
-    def chosen(d, x):
-        return (info[d, pl.ds(x, 1), :] == slot_id).astype(F32).astype(BF16)
 
     for copy in raw_in:
         copy.wait()
-    pl.semaphore_wait(barrier, n_ep + 1)
-
-    right, left = ep_at(1), ep_at(n_z - 1)
-    ring, infos = {}, {}
-    for d in (1, 3, 2):
-        infos[n_z - d] = send(info.at[0], info.at[n_z - d], ep=ep_at(d))
-    for a in (0, 1):
-        ring[3, a] = send(raw.at[0, a], raw.at[3, a], ep=right)
-    for a in (0, 1):
-        ring[1, a] = send(raw.at[0, a], raw.at[1, a], ep=left)
-
-    to_y, xed, cored, cored2 = {}, {}, {}, {}
-
-    def spread(src, a, key):
-        xed[key, a] = send(arr_a.at[p, src, a], arr_a.at[p, src, a], tp=p_x)
-
-    def pick(d, a):
-        src = ep_at(d)
-        if d:
-            picks = jnp.concatenate([chosen(d, e_y), chosen(d, e)], axis=0)
+    pl.semaphore_wait(barrier, 5 + is_mid.astype(jnp.int32))
+
+    def group_of(kind):
+        return RAW if kind[0] == "raw" else SMALL
+
+    def along(kind, ref, s):
+        if s == 0:
+            send((kind, "pair"), ref, ref, group_of(kind), ep=ep_of(z_pair), arrival=(kind, 1))
+
+            only(is_mid, "mid", lambda: send((kind, "mid"), ref, ref, group_of(kind),
+                                             ep=ep_of(z_mid), arrival=(kind, 2)))
+        elif s == 1:
+            send((kind, "mid1"), ref, ref, group_of(kind), ep=ep_of(z_mid), arrival=(kind, 3))
         else:
-            picks = chosen(d, e_y)
+            send((kind, "out", s), ref, ref, group_of(kind), ep=ep_of(z_pair), arrival=(kind, s))
+
+    along("info", info.at[z], 0)
+    along(("raw", 0), raw.at[z, 0], 0)
+    along(("raw", 1), raw.at[z, 1], 0)
+
+    def wide():
+        for a in (0, 1):
+            send(("wide", a), other_x.at[a], raw_x.at[a], RAW, ep=ep_of(z_pair))
+
+
+    def parts_of(s, a):
+        plane = planes[s]
+        own = [(("raw", a), raw.at[plane, a])]
+        if a == 0:
+            return [("info", info.at[plane])] + own
+        return own + [("gall", gall.at[ep_of(plane)])]
+
+    def pass_on(s, a):
+        for kind, ref in parts_of(s, a):
+            landed((kind, s), ref)
+            along(kind, ref, s)
+
+    def settle(s, a):
+        for kind, ref in parts_of(s, a):
+            landed((kind, s), ref)
+
+    def chosen(s, x):
+        return (info[planes[s], pl.ds(x, 1), :] == slot_id).astype(F32).astype(BF16)
+
+    def core(key, a, block, src):
+        ref = arr_a.at[block, src, a]
+        send((key, a), ref, ref, TO_CORE, tp=p_core, arrival=("c", key[1], a))
+
+    def pick(s, a, diagonal=1):
+        plane = planes[s]
+        src = ep_of(plane)
+        if s:
+            picks = jnp.concatenate([chosen(s, e_y), chosen(s, e)], axis=0)
+        else:
+            picks = chosen(s, e_y)
+        rows = contract(picks, raw[plane, a], ((1,), (0,))).astype(BF16)
+        ysa[plane, a] = rows[:cap]
+        there = arr_a.at[p, src, a]
+        send(("y", s, a), ysa.at[plane, a], there, TO_Y, ep=e_y)
+        if s:
+            if diagonal:
+                send(("x", s, 1, a), ysa.at[plane, a], there, TO_X, ep=e_y, tp=p_x)
+            arr_a[p, src, a] = rows[cap:]
+            send(("x", s, 0, a), there, there, TO_X, tp=p_x)
+            core(("c", s, 0), a, p, src)
+            if a == 1:
+                send(("gy", s), gall.at[src], gall.at[src], SMALL, ep=e_y)
+        else:
             ysx[a] = contract(picks, other_x[a], ((1,), (0,))).astype(BF16)
-        rows = contract(picks, raw[d, a], ((1,), (0,))).astype(BF16)
-        ysa[d, a] = rows[:cap]
-        to_y[d, a] = [send(ysa.at[d, a], arr_a.at[p, src, a], ep=e_y)]
-        if d:
-            arr_a[p, src, a] = rows[cap:]
-            spread(src, a, (d, 0))
-        else:
-            to_y[d, a].append(send(ysx.at[a], arr_a.at[p_x, src, a], ep=e_y))
-
-    def arrive(d, a):
-        ring[d, a].wait_recv()
-        if d == 3:
-            ring[2, a] = send(raw.at[3, a], raw.at[2, a], ep=right)
-        pick(d, a)
-
-    def from_y(d, a):
-        for copy in to_y[d, a]:
-            copy.wait_recv()
-        if d:
-            spread(ep_at(d, 1), a, (d, 1))
-
-    def to_core(d, h):
-        src = ep_at(d, h)
-        cored[d, h] = send(arr_a.at[p, src], arr_a.at[p, src], tp=p_core)
-
-    def x_to_core(d, h):
-        if d:
-            xed[(d, h), 0].wait_recv()
-            xed[(d, h), 1].wait_recv()
-        src = ep_at(d, h)
-        cored2[d, h] = send(arr_a.at[p_x, src], arr_a.at[p_x, src], tp=p_core)
-
-    pick(0, 0)
-    pick(0, 1)
-
-    for copy in full_in:
-        copy.wait()
-    for x in range(n_exp):
-        sel[x] = (place_t[x:x + 1, :] == slot_id).astype(F32).astype(BF16)
-    all_sel = sel[...].reshape(n_exp * cap, toks)
-    place = jnp.transpose(place_t)
-    member8 = place[:, :n_exp] > -1.0
-    logits = contract(tok[...], rw[...], ((1,), (1,)))
-    score = jnp.where(member8, jax.nn.sigmoid(logits), 0.0)
-    score_sum = jnp.sum(score, axis=1, keepdims=True)
-    gating = score / score_sum
-    lane_s = (lax.broadcasted_iota(jnp.int32, (toks, two), 1) - y * cap).astype(F32)
-
-    def hit(x):
-        return (place[:, x:x + 1] == lane_s).astype(F32)
-
-    for x in range(n_exp):
-        row = jnp.sum(hit(x) * gating[:, x:x + 1], axis=0, keepdims=True)
-        gs[x] = jnp.broadcast_to(row, (8, two))
-    gated = {}
-    for d, h in offsets:
-        other = ep_at(d, h)
-        gated[(n_z - d) % n_z, h] = send(gs.at[other], gr.at[e], ep=other)
-    gr[e] = gs[e]
-    own = sel[e]
-    for a, ref in enumerate((tok, cot)):
-        rows = contract(own, ref[...], ((1,), (0,))).astype(BF16)
-        for ref_b, b, start, size in pieces:
-            ref_b[b, e, a] = rows[:, start:start + size]
-
-    ret_c, ret_x, ret_f = {}, {}, {}
-
-    def base_of(q):
-        return ((z + q) % n_z) * 2
-
-    def compute(q):
-        for h in ((1,) if q == 0 else (0, 1)):
-            gated[q, h].wait_recv()
-            cored[q, h].wait_recv()
-            cored2[q, h].wait_recv()
-        base = base_of(q)
+            send(("yx", a), ysx.at[a], arr_a.at[p_x, src, a], TO_Y, ep=e_y, arrival=("y", 0, a))
+
+    def pick_wide(a):
+        src = ep_of(z_pair)
+        picks = jnp.concatenate([chosen(1, e_y), chosen(1, e)], axis=0)
+        for i, (block, source) in enumerate(((p, raw.at[z_pair, a]), (p_x, raw_x.at[a]))):
+            if i:
+                landed(("wide", a), raw_x.at[a])
+            rows = contract(picks, source[...], ((1,), (0,))).astype(BF16)
+            buffer = ysw.at[a] if i else ysa.at[z_pair, a]
+            buffer[...] = rows[:cap]
+            send(("yw", a, i), buffer, arr_a.at[block, src, a], TO_Y, ep=e_y, arrival=("yw", a))
+            arr_a[block, src, a] = rows[cap:]
+            core(("cw"[i], 1, 0), a, block, src)
+        if a == 1:
+            send(("gy", 1), gall.at[src], gall.at[src], SMALL, ep=e_y)
+
+    def from_y_wide(a):
+        src = ep_of(z_pair, 1)
+        landed(("yw", a), ysx)
+        core(("c", 1, 1), a, p, src)
+        core(("c2", 1, 1), a, p_x, src)
+
+    def from_y(s, a, diagonal=1):
+        src = ep_of(planes[s], 1)
+        landed(("y", s, a), arr_a.at[p, src, a] if s else ysx)
+        if not diagonal:
+            send(("x", s, 1, a), arr_a.at[p, src, a], arr_a.at[p, src, a], TO_X, tp=p_x)
+        core(("c", s, 1), a, p, src)
+        if s == 0:
+            core(("c2", s, 1), a, p_x, src)
+
+    def from_x(s, h, a):
+        src = ep_of(planes[s], h)
+        landed(("x", s, h, a), arr_a.at[p_x, src, a])
+        core(("c2", s, h), a, p_x, src)
+
+    def gathered(s, a):
+        landed(("c", s, a), arr_a.at[0, pl.ds(0, 2)] if s else ysx)
+
+    def compute_a(s):
+        gathered(s, 0)
+        pair = pl.ds(planes[s] * 2, 2)
+        pre = jnp.zeros((two, 2 * hid), F32)
+        for b in range(n_tp):
+            c = slice(b * fb, (b + 1) * fb)
+            pre = pre + contract(arr_a[b, pair, 0].reshape(two, fb), wgu[c, :], ((1,), (0,)))
+        pre_gate, pre_up = pre[:, :hid], pre[:, hid:]
+        activated, slope = silu_parts(pre_gate)
+        mid[s, 0] = activated
+        mid[s, 1] = pre_up * slope
+        mid[s, 2] = (activated * pre_up).astype(BF16).astype(F32)
+
+    def compute_b(s):
+        plane = planes[s]
+        base = plane * 2
+        gathered(s, 1)
+        landed(("gy", s), gall.at[ep_of(plane, 1)])
         pair = pl.ds(base, 2)
         here = pl.ds(pl.multiple_of(base * cap, two), two)
-        pre = jnp.zeros((two, 2 * hid), F32)
         back = jnp.zeros((two, hid), F32)
-        for ref_b, b, start, size in pieces:
-            c = slice(start, start + size)
-            pre = pre + contract(ref_b[b, pair, 0].reshape(two, size), wgu[c, :], ((1,), (0,)))
-            back = back + contract(ref_b[b, pair, 1].reshape(two, size), wd[:, c], ((1,), (1,)))
-        gate = jnp.transpose(gr[base] + gr[base + 1])[:, 0:1]
-        pre_gate, pre_up = pre[:, :hid], pre[:, hid:]
-        activated, slope = silu_parts(pre_gate)
-        hidden = (activated * pre_up).astype(BF16).astype(F32)
-        prod = hidden * back
-        ggb[base // 2] = contract(jnp.ones((8, hid), F32), prod, ((1,), (1,)),
-                                  lax.Precision.HIGHEST)
+        for b in range(n_tp):
+            c = slice(b * fb, (b + 1) * fb)
+            back = back + contract(arr_a[b, pair, 1].reshape(two, fb), wd[:, c], ((1,), (1,)))
+        gate = jnp.concatenate([jnp.sum(jnp.where(
+            gall[base + i, pl.ds(n_exp + e, 1), :] == slot_id, gall[base + i, pl.ds(e, 1), :], 0.0),
+            axis=1, keepdims=True) for i in (0, 1)], axis=0)
+        hidden = mid[s, 2]
         scaled = gate * back
-        grads = jnp.concatenate([(scaled * pre_up * slope).astype(BF16),
-                                 (scaled * activated).astype(BF16)], axis=1)
+        grads = jnp.concatenate([(scaled * mid[s, 1]).astype(BF16),
+                                 (scaled * mid[s, 0]).astype(BF16)], axis=1)
+        for i, b in ((1, p_both), (0, p_core)):
+            wb = wgu[pl.ds(pl.multiple_of(b * fb, 128), fb), :]
+            part[b, pair] = contract(grads, wb, ((1,), (1,))).astype(BF16).reshape(2, cap, fb)
+            send(("pc", s, i), part.at[b, pair], pc.at[i, pair], BACK, tp=p_core)
+        ggb[plane] = contract(jnp.ones((8, hid), F32), hidden * back, ((1,), (1,)),
+                              lax.Precision.HIGHEST)
+        send(("ggc", s), ggb.at[plane], ggc.at[plane], SMALL, tp=p_core)
+        for b in (p_x, p):
+            wb = wgu[pl.ds(pl.multiple_of(b * fb, 128), fb), :]
+            part[b, pair] = contract(grads, wb, ((1,), (1,))).astype(BF16).reshape(2, cap, fb)
         gp[here, :] = grads
         sh[here, :] = (gate * hidden).astype(BF16)
-        for b in range(n_tp):
-            part[b, pair] = contract(grads, wgu[b * fb:(b + 1) * fb, :], ((1,), (1,))).astype(
-                BF16).reshape(2, cap, fb)
-        ret_c[q] = (send(part.at[p_both, pair], pc.at[1, pair], tp=p_core),
-                    send(part.at[p_core, pair], pc.at[0, pair], tp=p_core))
-
-    def to_x(q):
-        pair = pl.ds(base_of(q), 2)
-        ret_c[q][0].wait_recv()
+
+    def gate_home(s):
+        plane = planes[s]
+        landed(("ggc", s), ggc.at[plane])
+        ggs[plane] = ggb[plane] + ggc[plane]
+        for h in (0, 1):
+            for far, tp in ((0, p), (1, p_x)):
+                if s == 0 and h == 0 and far == 0:
+                    ggh[e, x_me] = ggs[plane]
+                else:
+                    send(("ggh", s, h, far), ggs.at[plane], ggh.at[e, x_me], SMALL,
+                         ep=ep_of(plane, h), tp=tp, arrival="ggh" if s or h else "ggh2")
+
+    def to_x(s):
+        pair = pl.ds(planes[s] * 2, 2)
+        landed(("pc", s, 1), pc.at[1, pair])
         xs[pair] = (part[p_x, pair].astype(F32) + pc[1, pair].astype(F32)).astype(BF16)
-        ret_x[q] = send(xs.at[pair], xr.at[pair], tp=p_x)
-
-    def to_home(q):
-        pair = pl.ds(base_of(q), 2)
-        ret_c[q][1].wait_recv()
-        ret_x[q].wait_recv()
-        fin[pair] = (part[p, pair].astype(F32) + pc[0, pair].astype(F32)
-                     + xr[pair].astype(F32)).astype(BF16)
-        for h in ((1,) if q == 0 else (0, 1)):
-            other = ep_at(q, h)
-            ret_f[q, h] = send(fin.at[other], home.at[e], ep=other)
-        if q == 0:
+        for h in (0, 1):
+            src = ep_of(planes[s], h)
+            send(("xs", s, h), xs.at[src], xr.at[src], BACK, tp=p_x)
+        landed(("pc", s, 0), pc.at[0, pair])
+
+    def to_home(s, h):
+        other = ep_of(planes[s], h)
+        landed(("xs", s, h), xr.at[other])
+        fin[other] = (part[p, other].astype(F32) + pc[0, other].astype(F32)
+                      + xr[other].astype(F32)).astype(BF16)
+        if s or h:
+            send(("fin", s, h), fin.at[other], home.at[e], HOME, ep=other, arrival="fin")
+        else:
             home[e] = fin[e]
 
-    for d in (3, 1, 2):
-        infos[d].wait_recv()
-    from_y(0, 0)
-    from_y(0, 1)
-    to_core(0, 1)
-    x_to_core(0, 1)
-    arrive(3, 0)
-    from_y(3, 0)
-    arrive(3, 1)
-    to_core(3, 0)
-    from_y(3, 1)
-    to_core(3, 1)
-    for copy in weights_in:
-        copy.wait()
-    compute(0)
-    arrive(1, 0)
-    x_to_core(3, 0)
-    from_y(1, 0)
-    to_x(0)
-    arrive(1, 1)
-    to_core(1, 0)
-    x_to_core(3, 1)
-    from_y(1, 1)
-    to_core(1, 1)
-    compute(3)
-    to_home(0)
-    arrive(2, 0)
-    from_y(2, 0)
-    x_to_core(1, 0)
-    to_x(3)
-    arrive(2, 1)
-    to_core(2, 0)
-    x_to_core(1, 1)
-    from_y(2, 1)
-    to_core(2, 1)
-    compute(1)
-    to_home(3)
-    x_to_core(2, 0)
-    x_to_core(2, 1)
-    to_x(1)
-    compute(2)
-    last = 2
-    gg_c = send(ggb, ggc, tp=p_core)
-    to_x(last)
-    gg_c.wait_recv()
-    ggb2 = ggb[...] + ggc[...]
-    ggc[...] = ggb2
-    gg_x = send(ggc, ggx, tp=p_x)
-    to_home(1)
-    grads = gp[...]
-
-    def in_block(i):
-        ref_b, b, start, size = pieces[i]
-        rows = ref_b[b, :, 0].reshape(n_ep * cap, size)
-        sums = contract(grads, rows, ((0,), (0,)))
-        c = slice(start, start + size)
+    def in_block(b):
+        rows = arr_a[b, :, 0].reshape(n_ep * cap, fb)
+        sums = contract(gp[...], rows, ((0,), (0,)))
+        c = slice(b * fb, (b + 1) * fb)
         o_gate[c, :] = jnp.transpose(sums[:hid]).astype(BF16)
         o_up[c, :] = jnp.transpose(sums[hid:]).astype(BF16)
         nb[0:1, c] = jnp.sum(sums[:hid] * sums[:hid], axis=0, keepdims=True)
         nb[1:2, c] = jnp.sum(sums[hid:] * sums[hid:], axis=0, keepdims=True)
 
-    in_block(0)
-    gg_x.wait_recv()
-    ggx[...] = ggb2 + ggx[...]
-    gg_f = {}
-    for k in offsets:
-        other = ep_at(*k)
-        gg_f[k] = send(ggx.at[other // 2], ggh.at[e], ep=other)
-    ggh[e] = ggx[e // 2]
-    in_block(1)
-    to_home(last)
-    for i in range(2, len(pieces)):
-        in_block(i)
-    nb_c = send(nb, nc, tp=p_core)
-
-    for k in offsets:
-        gg_f[k].wait_recv()
-    lane8 = lax.broadcasted_iota(jnp.int32, (toks, n_exp), 1)
-    got = jnp.zeros((toks, n_exp), F32)
+    def down():
+        dn = jnp.zeros((hid, 1), F32)
+        for b in range(n_tp):
+            sums = contract(sh[...], arr_a[b, :, 1].reshape(n_ep * cap, fb), ((0,), (0,)))
+            o_down[:, b * fb:(b + 1) * fb] = sums.astype(BF16)
+            dn = dn + jnp.sum(sums * sums, axis=1, keepdims=True)
+        o_dnorm[...] = jnp.transpose(jnp.broadcast_to(dn, (hid, 128)))[0:1, :]
+
+    pick(0, 0)
+    pick(0, 1)
+
+    for copy in full_in[:2]:
+        copy.wait()
+    logits_t = contract(rw[...], tok[...], ((1,), (1,)))
+    score_t = jnp.where(member_t, jax.nn.sigmoid(logits_t), 0.0)
+    score_sum = jnp.sum(score_t, axis=0, keepdims=True)
+    gating_t = score_t / score_sum
+    gall[e, 0:n_exp] = gating_t
+    gall[e, n_exp:2 * n_exp] = place_t
+    along("gall", gall.at[e], 0)
+    only(is_edge, "edge", wide)
+    send(("gy", 0), gall.at[e], gall.at[e], SMALL, ep=e_y)
     for x in range(n_exp):
-        col = jnp.sum(hit(x) * ggh[x, 0:1, :], axis=1, keepdims=True)
-        got = got + jnp.where(lane8 == x, col, 0.0)
-    got_t = jnp.transpose(jnp.concatenate(
-        [got, jnp.zeros((toks, 128 - n_exp), F32)], axis=1))[:n_exp]
+        sel[x] = (place_t[x:x + 1, :] == slot_id).astype(F32).astype(BF16)
+    full_in[2].wait()
+    for a, ref in enumerate((tok, cot)):
+        rows = contract(sel[e], ref[...], ((1,), (0,))).astype(BF16)
+        for b in range(n_tp):
+            arr_a[b, e, a] = rows[:, b * fb:(b + 1) * fb]
+    for copy in weights_in:
+        copy.wait()
+
+    def mid_plane():
+        pass_on(1, 0)
+        pass_on(2, 0)
+        pick(2, 0)
+        pass_on(1, 1)
+        pass_on(2, 1)
+        pick(2, 1)
+        from_y(0, 0)
+        from_y(0, 1)
+        compute_a(0)
+        pass_on(3, 0)
+        pick(3, 0)
+        compute_b(0)
+        from_x(2, 0, 0)
+        from_y(2, 0)
+        from_x(2, 1, 0)
+        gate_home(0)
+        pass_on(3, 1)
+        pick(3, 1)
+        pick_wide(0)
+        pick_wide(1)
+        from_x(2, 0, 1)
+        from_y(2, 1)
+        from_x(2, 1, 1)
+        compute_a(2)
+        compute_b(2)
+        from_x(3, 0, 0)
+        from_y(3, 0)
+        from_x(3, 1, 0)
+        gate_home(2)
+        to_x(2)
+        to_x(0)
+        compute_a(3)
+        from_x(3, 0, 1)
+        from_y(3, 1)
+        from_x(3, 1, 1)
+        compute_b(3)
+        to_home(2, 0)
+        from_y_wide(0)
+        to_home(2, 1)
+        gate_home(3)
+        to_x(3)
+        compute_a(1)
+        from_y_wide(1)
+        compute_b(1)
+        to_home(3, 0)
+        in_block(0)
+        in_block(1)
+        to_home(3, 1)
+        gate_home(1)
+        to_x(1)
+        in_block(2)
+        in_block(3)
+        send("nbc", nb, nc, SMALL, tp=p_core)
+        down()
+        landed("nbc", nc)
+        nc[...] = nb[...] + nc[...]
+        send("nbx", nc, nx, SMALL, tp=p_x)
+        to_home(1, 0)
+        to_home(1, 1)
+
+    def edge_plane():
+        settle(1, 0)
+        pick(1, 0, 0)
+        settle(1, 1)
+        pick(1, 1, 0)
+        from_y(1, 0, 0)
+        settle(2, 0)
+        pick(2, 0)
+        from_y(1, 1, 0)
+        from_y(0, 0)
+        from_y(0, 1)
+        compute_a(0)
+        settle(2, 1)
+        pick(2, 1)
+        compute_b(0)
+        from_x(1, 0, 0)
+        from_x(1, 1, 0)
+        gate_home(0)
+        from_x(1, 0, 1)
+        compute_a(1)
+        settle(3, 0)
+        pick(3, 0)
+        from_x(1, 1, 1)
+        from_x(2, 0, 0)
+        from_y(2, 0)
+        compute_b(1)
+        settle(3, 1)
+        pick(3, 1)
+        from_x(2, 1, 0)
+        gate_home(1)
+        to_x(1)
+        compute_a(2)
+        from_x(2, 0, 1)
+        from_y(2, 1)
+        from_x(2, 1, 1)
+        compute_b(2)
+        from_x(3, 0, 0)
+        from_y(3, 0)
+        from_x(3, 1, 0)
+        gate_home(2)
+        to_x(2)
+        compute_a(3)
+        from_x(3, 0, 1)
+        from_y(3, 1)
+        from_x(3, 1, 1)
+        to_home(1, 0)
+        compute_b(3)
+        to_home(1, 1)
+        in_block(0)
+        gate_home(3)
+        to_x(3)
+        to_x(0)
+        to_home(2, 0)
+        in_block(1)
+        to_home(2, 1)
+        in_block(2)
+        in_block(3)
+        send("nbc", nb, nc, SMALL, tp=p_core)
+        down()
+        to_home(3, 0)
+        landed("nbc", nc)
+        nc[...] = nb[...] + nc[...]
+        send("nbx", nc, nx, SMALL, tp=p_x)
+        to_home(3, 1)
+
+    only(is_mid, "mid", mid_plane)
+    only(is_edge, "edge", edge_plane)
+
+
+    landed("ggh", ggh.at[pl.ds(0, n_exp - 1)])
+    landed("ggh2", ggh.at[0, 0])
+    gts[0:n_exp, :] = ggh[:, 0, 0, :] + ggh[:, 1, 0, :]
+    gts[...] = jnp.transpose(gts[...])
+    mine = gts[pl.ds(pl.multiple_of(y * cap, 8), cap), :]
+    got_t = jnp.concatenate([jnp.sum(jnp.where(
+        place_t[x:x + 1, :] == slot_id, mine[:, x:x + 1], 0.0), axis=0, keepdims=True)
+        for x in range(n_exp)], axis=0)
     for k, r in enumerate((r0, r1)):
         o_gg[k:k + 1, :] = jnp.sum(jnp.where(r == row_e[:n_exp], got_t, 0.0), axis=0, keepdims=True)
-    weighted = jnp.sum(gating * got, axis=1, keepdims=True)
-    grad_logits = jnp.where(member8, (got - weighted) / score_sum * score * (1.0 - score),
+    weighted = jnp.sum(gating_t * got_t, axis=0, keepdims=True)
+    grad_logits = jnp.where(member_t, (got_t - weighted) / score_sum * score_t * (1.0 - score_t),
                             0.0).astype(BF16)
-    rp[...] = contract(grad_logits, tok[...], ((0,), (0,)))
+    rp[...] = contract(grad_logits, tok[...], ((1,), (0,)))
     span = width // n_ep
-    rr_f = {}
-    for k in offsets:
-        other = ep_at(*k)
-        rr_f[k] = send(rp.at[:, pl.ds(pl.multiple_of(other * span, 128), span)], rr.at[e], ep=other)
+    for s in (3, 2, 1, 0):
+        for h in (0, 1):
+            if s or h:
+                other = ep_of(planes[s], h)
+                send(("rr", s, h), rp.at[:, pl.ds(pl.multiple_of(other * span, 128), span)],
+                     rr.at[e], SMALL, ep=other, arrival="rr")
     rr[e] = rp[:, pl.ds(pl.multiple_of(e * span, 128), span)]
-    nb_c.wait_recv()
-    nc[...] = nb[...] + nc[...]
-    nb_x = send(nc, nx, tp=p_x)
-    shv = sh[...]
-    dn = jnp.zeros((hid, 1), F32)
-    for ref_b, b, start, size in pieces:
-        sums = contract(shv, ref_b[b, :, 1].reshape(n_ep * cap, size), ((0,), (0,)))
-        o_down[:, start:start + size] = sums.astype(BF16)
-        dn = dn + jnp.sum(sums * sums, axis=1, keepdims=True)
-    o_dnorm[...] = jnp.transpose(jnp.broadcast_to(dn, (hid, 128)))[0:1, :]
-    router_term = contract(grad_logits, rw[:, cols], ((1,), (0,)))
-    nb_x.wait_recv()
+    to_home(0, 1)
+    to_home(0, 0)
+    landed("nbx", nx)
     o_norm[...] = nc[...] + nx[...]
-    for k in offsets:
-        rr_f[k].wait_recv()
+    landed("fin", home.at[pl.ds(0, n_ep - 1)])
+    landed("rr", rr.at[pl.ds(0, n_ep - 1)])
     total = rr[0]
     for x in range(1, n_ep):
         total = total + rr[x]
     o_gr[...] = total
     o_rnorm[...] = jnp.sum(total * total, axis=0, keepdims=True)
-    for k in offsets:
-        ret_f[k].wait_recv()
+    router_term = contract(grad_logits, rw[:, cols], ((0,), (0,)))
+    all_sel = sel[...].reshape(n_exp * cap, toks)
     o_tok[...] = (contract(all_sel, home[...].reshape(n_exp * cap, fb), ((0,), (0,)))
                   + router_term).astype(BF16)
-    for copy in started:
-        copy.wait_send()
+    def drain(name):
+        for group in range(SMALL + 1):
+            count = sum(n for (where, _), (g, n) in sends.items()
+                        if g == group and where in ("all", name))
+            if group == SMALL:
+                d = next(d for d in (4, 2, 1) if count % d == 0)
+                whole = mid.at[pl.ds(0, d), 0, pl.ds(0, count // d * n_exp)]
+            else:
+                d, k, j = next((d, k, j) for d in range(1, n_tp + 1) for j in (1, 2)
+                               for k in range(1, n_ep + 1) if d * k * j == count)
+                whole = arr_a.at[pl.ds(0, d), pl.ds(0, k), pl.ds(0, j)]
+            transfer(group, "fin", whole, whole).wait_send()
+
+    only(is_edge, "edge", lambda: drain("edge"))
+    only(is_mid, "mid", lambda: drain("mid"))
 
 
 def flush(*refs):
@@ -537,7 +700,6 @@
     two = 2 * cap
     slots = n_ep * cap
     span = width // n_ep
-    copies = 16 * n_ep
     results = [
         ((toks, fb), BF16),
         ((routing.shape[1], toks), F32),
@@ -567,11 +729,13 @@
             pltpu.VMEM((n_ep // 2, 2, toks, fb), BF16),
             pltpu.VMEM((n_ep // 2, n_exp, toks), F32),
             pltpu.VMEM((2, toks, fb), BF16),
+            pltpu.VMEM((2, toks, fb), BF16),
             pltpu.VMEM((n_ep // 2, 2, cap, fb), BF16),
             pltpu.VMEM((2, cap, fb), BF16),
+            pltpu.VMEM((2, cap, fb), BF16),
             pltpu.VMEM((n_tp, n_ep, 2, cap, fb), BF16),
-            pltpu.VMEM((n_exp, 8, two), F32),
-            pltpu.VMEM((n_ep, 8, two), F32),
+            pltpu.VMEM((n_ep, 2 * n_exp, toks), F32),
+            pltpu.VMEM((n_ep // 2, 3, two, hid), F32),
             pltpu.VMEM((n_tp, n_ep, cap, fb), BF16),
             pltpu.VMEM((2, n_ep, cap, fb), BF16),
             pltpu.VMEM((n_ep, cap, fb), BF16),
@@ -583,15 +747,16 @@
             pltpu.VMEM((n_ep // 2, 8, two), F32),
             pltpu.VMEM((n_ep // 2, 8, two), F32),
             pltpu.VMEM((n_ep // 2, 8, two), F32),
-            pltpu.VMEM((n_exp, 8, two), F32),
+            pltpu.VMEM((n_exp, 2, 8, two), F32),
+            pltpu.VMEM((two, toks), F32),
             pltpu.VMEM((2, width), F32),
             pltpu.VMEM((2, width), F32),
             pltpu.VMEM((2, width), F32),
             pltpu.VMEM((n_exp, width), F32),
             pltpu.VMEM((n_ep, n_exp, span), F32),
             pltpu.SemaphoreType.DMA((11,)),
-            pltpu.SemaphoreType.DMA((copies,)),
-            pltpu.SemaphoreType.DMA((copies,)),
+            pltpu.SemaphoreType.DMA((SMALL + 1,)),
+            pltpu.SemaphoreType.DMA((80,)),
         ],
         compiler_params=pltpu.CompilerParams(
             collective_id=0, has_side_effects=True, vmem_limit_bytes=40 << 20

time: 62.9 us -> 51 us (0.81)
  Pallas kernels: 62.1 us -> 50 us
    pallas_call x1, Pallas kernels: 60.8 us -> 48.7 us  [fused(): pl.pallas_call(functools.partial(kernel, n_ep, n_tp, cap), out_shape=[plt...]
where the time goes in v2:
time: 51 us; the launch traced here: 50.8 us
  Pallas kernels  50 us (98%)
  between operations  0.81 us (2%)
    pallas_call x1, Pallas kernels, fused(): pl.pallas_call(functools.partial(kernel, n_ep, n_tp, cap), out_shape=[plt...  48.7 us
    pallas_call x1, Pallas kernels, fused(): pl.pallas_call(flush, out_shape=[jax.ShapeDtypeStruct(shape, dtype) for s...  1.28 us

profile of v2, /device:TPU:0, one launch (start us, length us, event | category | flops | bytes accessed | tf_op | source)
XLA Modules:
  0.0 50.8 jit_solution(6541539913128683985)
XLA Ops:
  0.6 48.7 %shard_map.142 = (bf16[128,512]{1,0:T(8,128)(2,1)S(1)}, f32[2,128]{1,0:T(2,128)S(1)}, f32[8,256]{1,0:T(8,128)S(1)}, bf16[2048,128]{1,0:T(8,128)(2,1)S(1)}, bf16[...) custom-call(bf16[128,2048]{1,0:T(8,128)(2,1)} %tok_hbm.1, ...), custom_call_target="tpu_custom_call" | custom-call | tf_op jit(solution)/shard_map/pallas_call | solution.py:716
  49.4 1.3 %shard_map.143 = (bf16[128,512]{1,0:T(8,128)(2,1)}, f32[2,128]{1,0:T(2,128)}, f32[8,256]{1,0:T(8,128)}, bf16[2048,128]{1,0:T(8,128)(2,1)}, bf16[2048,128]{1,0:T(...) custom-call(bf16[128,512]{1,0:T(8,128)(2,1)S(1)} %get-tuple-element.27.refs_0_, ...), custom_call_target="tpu_custom_call" | custom-call | tf_op jit(solution)/shard_map/pallas_call | solution.py:767

commit v3 on v2

--- a/solution.py
+++ b/solution.py
@@ -188,7 +188,7 @@
            tok_hbm, cot_hbm, rt_hbm, rw_hbm, wg, wu, wd_hbm,
            o_tok, o_gg, o_gr, o_gate, o_up, o_down, o_norm, o_dnorm, o_rnorm,
            rt, rw, tok, cot, wgu, wd, sel, raw, info, other_x, raw_x, ysa, ysx, ysw, arr_a, gall, mid, part, pc, xs, xr,
-           fin, home, gp, sh, ggb, ggc, ggs, ggh, gts, nb, nc, nx, rp, rr, lsem, ssem, rsem):
+           fin, home, gp, sh, ggb, ggc, ggs, ggh, gts, nb, nc, nx, gl, rp, rr, lsem, ssem, rsem, ready):
     e = lax.axis_index("ep")
     p = lax.axis_index("tp")
     z, y = e // 2, e % 2
@@ -246,7 +246,7 @@
     def _():
         pl.semaphore_signal(barrier, inc=1, device_id=(ep_of(z_mid), p), device_id_type=MESH)
 
-    for ep, tp in ((e_y, p_x), (e_y, p), (e, p_x), (e, p_core)):
+    for ep, tp in ((e_y, p), (e, p_x), (e, p_core)):
         pl.semaphore_signal(barrier, inc=1, device_id=(ep, tp), device_id_type=MESH)
     routing_in = load(rt_hbm, rt)
     cols = pl.ds(pl.multiple_of(p * fb, 128), fb)
@@ -270,9 +270,8 @@
     info[z] = place_t
     slot_id = lax.broadcasted_iota(jnp.int32, (cap, toks), 0).astype(F32)
 
-    for copy in raw_in:
-        copy.wait()
-    pl.semaphore_wait(barrier, 5 + is_mid.astype(jnp.int32))
+    raw_in[0].wait()
+    pl.semaphore_wait(barrier, 4 + is_mid.astype(jnp.int32))
 
     def group_of(kind):
         return RAW if kind[0] == "raw" else SMALL
@@ -290,7 +289,11 @@
 
     along("info", info.at[z], 0)
     along(("raw", 0), raw.at[z, 0], 0)
+    raw_in[1].wait()
     along(("raw", 1), raw.at[z, 1], 0)
+    pl.semaphore_signal(ready, inc=1, device_id=(e, p_x), device_id_type=MESH)
+    for copy in raw_in[2:]:
+        copy.wait()
 
     def wide():
         for a in (0, 1):
@@ -323,6 +326,8 @@
     def pick(s, a, diagonal=1):
         plane = planes[s]
         src = ep_of(plane)
+        if s and a:
+            send(("gy", s), gall.at[src], gall.at[src], SMALL, ep=e_y)
         if s:
             picks = jnp.concatenate([chosen(s, e_y), chosen(s, e)], axis=0)
         else:
@@ -337,14 +342,14 @@
             arr_a[p, src, a] = rows[cap:]
             send(("x", s, 0, a), there, there, TO_X, tp=p_x)
             core(("c", s, 0), a, p, src)
-            if a == 1:
-                send(("gy", s), gall.at[src], gall.at[src], SMALL, ep=e_y)
         else:
             ysx[a] = contract(picks, other_x[a], ((1,), (0,))).astype(BF16)
             send(("yx", a), ysx.at[a], arr_a.at[p_x, src, a], TO_Y, ep=e_y, arrival=("y", 0, a))
 
     def pick_wide(a):
         src = ep_of(z_pair)
+        if a == 0:
+            send(("gy", 1), gall.at[src], gall.at[src], SMALL, ep=e_y)
         picks = jnp.concatenate([chosen(1, e_y), chosen(1, e)], axis=0)
         for i, (block, source) in enumerate(((p, raw.at[z_pair, a]), (p_x, raw_x.at[a]))):
             if i:
@@ -355,8 +360,6 @@
             send(("yw", a, i), buffer, arr_a.at[block, src, a], TO_Y, ep=e_y, arrival=("yw", a))
             arr_a[block, src, a] = rows[cap:]
             core(("cw"[i], 1, 0), a, block, src)
-        if a == 1:
-            send(("gy", 1), gall.at[src], gall.at[src], SMALL, ep=e_y)
 
     def from_y_wide(a):
         src = ep_of(z_pair, 1)
@@ -394,20 +397,26 @@
         mid[s, 1] = pre_up * slope
         mid[s, 2] = (activated * pre_up).astype(BF16).astype(F32)
 
+    def gates(s):
+        base = planes[s] * 2
+        landed(("gy", s), gall.at[ep_of(planes[s], 1)])
+        for i in (0, 1):
+            row = gall[base + i, pl.ds(e, 1), :]
+            hit = gall[base + i, pl.ds(n_exp + e, 1), :] == slot_id
+            column = jnp.sum(jnp.where(hit, row, 0.0), axis=1, keepdims=True)
+            mid[s, 3, i * cap:(i + 1) * cap] = jnp.broadcast_to(column, (cap, hid))
+
     def compute_b(s):
         plane = planes[s]
         base = plane * 2
         gathered(s, 1)
-        landed(("gy", s), gall.at[ep_of(plane, 1)])
         pair = pl.ds(base, 2)
         here = pl.ds(pl.multiple_of(base * cap, two), two)
         back = jnp.zeros((two, hid), F32)
         for b in range(n_tp):
             c = slice(b * fb, (b + 1) * fb)
             back = back + contract(arr_a[b, pair, 1].reshape(two, fb), wd[:, c], ((1,), (1,)))
-        gate = jnp.concatenate([jnp.sum(jnp.where(
-            gall[base + i, pl.ds(n_exp + e, 1), :] == slot_id, gall[base + i, pl.ds(e, 1), :], 0.0),
-            axis=1, keepdims=True) for i in (0, 1)], axis=0)
+        gate = mid[s, 3]
         hidden = mid[s, 2]
         scaled = gate * back
         grads = jnp.concatenate([(scaled * mid[s, 1]).astype(BF16),
@@ -441,7 +450,7 @@
         pair = pl.ds(planes[s] * 2, 2)
         landed(("pc", s, 1), pc.at[1, pair])
         xs[pair] = (part[p_x, pair].astype(F32) + pc[1, pair].astype(F32)).astype(BF16)
-        for h in (0, 1):
+        for h in ((0, 1) if s else (1, 0)):
             src = ep_of(planes[s], h)
             send(("xs", s, h), xs.at[src], xr.at[src], BACK, tp=p_x)
         landed(("pc", s, 0), pc.at[0, pair])
@@ -496,6 +505,32 @@
             arr_a[b, e, a] = rows[:, b * fb:(b + 1) * fb]
     for copy in weights_in:
         copy.wait()
+    pl.semaphore_wait(ready, 1)
+
+    def router():
+        landed("ggh", ggh.at[pl.ds(0, n_exp - 1)])
+        landed("ggh2", ggh.at[0, 0])
+        gts[0:n_exp, :] = ggh[:, 0, 0, :] + ggh[:, 1, 0, :]
+        gts[...] = jnp.transpose(gts[...])
+        mine = gts[pl.ds(pl.multiple_of(y * cap, 8), cap), :]
+        got_t = jnp.concatenate([jnp.sum(jnp.where(
+            place_t[x:x + 1, :] == slot_id, mine[:, x:x + 1], 0.0), axis=0, keepdims=True)
+            for x in range(n_exp)], axis=0)
+        for k, r in enumerate((r0, r1)):
+            o_gg[k:k + 1, :] = jnp.sum(jnp.where(r == row_e[:n_exp], got_t, 0.0), axis=0, keepdims=True)
+        weighted = jnp.sum(gating_t * got_t, axis=0, keepdims=True)
+        grad_logits = jnp.where(member_t, (got_t - weighted) / score_sum * score_t * (1.0 - score_t),
+                                0.0).astype(BF16)
+        gl[...] = grad_logits
+        rp[...] = contract(grad_logits, tok[...], ((1,), (0,)))
+        span = width // n_ep
+        for s in (3, 2, 1, 0):
+            for h in (1, 0):
+                if s or h:
+                    other = ep_of(planes[s], h)
+                    send(("rr", s, h), rp.at[:, pl.ds(pl.multiple_of(other * span, 128), span)],
+                         rr.at[e], SMALL, ep=other, arrival="rr")
+        rr[e] = rp[:, pl.ds(pl.multiple_of(e * span, 128), span)]
 
     def mid_plane():
         pass_on(1, 0)
@@ -509,6 +544,7 @@
         compute_a(0)
         pass_on(3, 0)
         pick(3, 0)
+        gates(0)
         compute_b(0)
         from_x(2, 0, 0)
         from_y(2, 0)
@@ -520,6 +556,7 @@
         pick_wide(1)
         from_x(2, 0, 1)
         from_y(2, 1)
+        gates(2)
         from_x(2, 1, 1)
         compute_a(2)
         compute_b(2)
@@ -532,6 +569,7 @@
         compute_a(3)
         from_x(3, 0, 1)
         from_y(3, 1)
+        gates(3)
         from_x(3, 1, 1)
         compute_b(3)
         to_home(2, 0)
@@ -540,6 +578,7 @@
         gate_home(3)
         to_x(3)
         compute_a(1)
+        gates(1)
         from_y_wide(1)
         compute_b(1)
         to_home(3, 0)
@@ -557,63 +596,70 @@
         send("nbx", nc, nx, SMALL, tp=p_x)
         to_home(1, 0)
         to_home(1, 1)
+        router()
+        to_home(0, 1)
+        to_home(0, 0)
 
     def edge_plane():
         settle(1, 0)
-        pick(1, 0, 0)
+        pick(1, 0)
         settle(1, 1)
-        pick(1, 1, 0)
-        from_y(1, 0, 0)
+        pick(1, 1)
         settle(2, 0)
-        pick(2, 0)
-        from_y(1, 1, 0)
+        pick(2, 0, 0)
         from_y(0, 0)
         from_y(0, 1)
+        gates(0)
         compute_a(0)
+        from_y(1, 0)
         settle(2, 1)
         pick(2, 1)
         compute_b(0)
         from_x(1, 0, 0)
         from_x(1, 1, 0)
-        gate_home(0)
+        from_y(1, 1)
         from_x(1, 0, 1)
+        from_x(1, 1, 1)
+        from_y(2, 0, 0)
+        gates(1)
         compute_a(1)
         settle(3, 0)
         pick(3, 0)
-        from_x(1, 1, 1)
-        from_x(2, 0, 0)
-        from_y(2, 0)
         compute_b(1)
         settle(3, 1)
         pick(3, 1)
+        from_x(2, 0, 0)
+        from_y(2, 1)
+        from_x(2, 0, 1)
         from_x(2, 1, 0)
+        gate_home(0)
         gate_home(1)
         to_x(1)
+        gates(2)
+        from_x(2, 1, 1)
         compute_a(2)
-        from_x(2, 0, 1)
-        from_y(2, 1)
-        from_x(2, 1, 1)
         compute_b(2)
+        from_y(3, 0)
         from_x(3, 0, 0)
-        from_y(3, 0)
         from_x(3, 1, 0)
+        gates(3)
+        compute_a(3)
         gate_home(2)
         to_x(2)
-        compute_a(3)
+        from_y(3, 1)
         from_x(3, 0, 1)
-        from_y(3, 1)
         from_x(3, 1, 1)
+        compute_b(3)
         to_home(1, 0)
-        compute_b(3)
-        to_home(1, 1)
         in_block(0)
+        in_block(1)
         gate_home(3)
         to_x(3)
         to_x(0)
+        to_home(1, 1)
         to_home(2, 0)
-        in_block(1)
+        in_block(2)
         to_home(2, 1)
-        in_block(2)
         in_block(3)
         send("nbc", nb, nc, SMALL, tp=p_core)
         down()
@@ -622,35 +668,14 @@
         nc[...] = nb[...] + nc[...]
         send("nbx", nc, nx, SMALL, tp=p_x)
         to_home(3, 1)
+        router()
+        to_home(0, 1)
+        to_home(0, 0)
 
     only(is_mid, "mid", mid_plane)
     only(is_edge, "edge", edge_plane)
 
 
-    landed("ggh", ggh.at[pl.ds(0, n_exp - 1)])
-    landed("ggh2", ggh.at[0, 0])
-    gts[0:n_exp, :] = ggh[:, 0, 0, :] + ggh[:, 1, 0, :]
-    gts[...] = jnp.transpose(gts[...])
-    mine = gts[pl.ds(pl.multiple_of(y * cap, 8), cap), :]
-    got_t = jnp.concatenate([jnp.sum(jnp.where(
-        place_t[x:x + 1, :] == slot_id, mine[:, x:x + 1], 0.0), axis=0, keepdims=True)
-        for x in range(n_exp)], axis=0)
-    for k, r in enumerate((r0, r1)):
-        o_gg[k:k + 1, :] = jnp.sum(jnp.where(r == row_e[:n_exp], got_t, 0.0), axis=0, keepdims=True)
-    weighted = jnp.sum(gating_t * got_t, axis=0, keepdims=True)
-    grad_logits = jnp.where(member_t, (got_t - weighted) / score_sum * score_t * (1.0 - score_t),
-                            0.0).astype(BF16)
-    rp[...] = contract(grad_logits, tok[...], ((1,), (0,)))
-    span = width // n_ep
-    for s in (3, 2, 1, 0):
-        for h in (0, 1):
-            if s or h:
-                other = ep_of(planes[s], h)
-                send(("rr", s, h), rp.at[:, pl.ds(pl.multiple_of(other * span, 128), span)],
-                     rr.at[e], SMALL, ep=other, arrival="rr")
-    rr[e] = rp[:, pl.ds(pl.multiple_of(e * span, 128), span)]
-    to_home(0, 1)
-    to_home(0, 0)
     landed("nbx", nx)
     o_norm[...] = nc[...] + nx[...]
     landed("fin", home.at[pl.ds(0, n_ep - 1)])
@@ -660,7 +685,7 @@
         total = total + rr[x]
     o_gr[...] = total
     o_rnorm[...] = jnp.sum(total * total, axis=0, keepdims=True)
-    router_term = contract(grad_logits, rw[:, cols], ((0,), (0,)))
+    router_term = contract(gl[...], rw[:, cols], ((0,), (0,)))
     all_sel = sel[...].reshape(n_exp * cap, toks)
     o_tok[...] = (contract(all_sel, home[...].reshape(n_exp * cap, fb), ((0,), (0,)))
                   + router_term).astype(BF16)
@@ -735,7 +760,7 @@
             pltpu.VMEM((2, cap, fb), BF16),
             pltpu.VMEM((n_tp, n_ep, 2, cap, fb), BF16),
             pltpu.VMEM((n_ep, 2 * n_exp, toks), F32),
-            pltpu.VMEM((n_ep // 2, 3, two, hid), F32),
+            pltpu.VMEM((n_ep // 2, 4, two, hid), F32),
             pltpu.VMEM((n_tp, n_ep, cap, fb), BF16),
             pltpu.VMEM((2, n_ep, cap, fb), BF16),
             pltpu.VMEM((n_ep, cap, fb), BF16),
@@ -752,11 +777,13 @@
             pltpu.VMEM((2, width), F32),
             pltpu.VMEM((2, width), F32),
             pltpu.VMEM((2, width), F32),
+            pltpu.VMEM((n_exp, toks), BF16),
             pltpu.VMEM((n_exp, width), F32),
             pltpu.VMEM((n_ep, n_exp, span), F32),
             pltpu.SemaphoreType.DMA((11,)),
             pltpu.SemaphoreType.DMA((SMALL + 1,)),
             pltpu.SemaphoreType.DMA((80,)),
+            pltpu.SemaphoreType.REGULAR,
         ],
         compiler_params=pltpu.CompilerParams(
             collective_id=0, has_side_effects=True, vmem_limit_bytes=40 << 20

time: 51 us -> 49.8 us (0.976)
  Pallas kernels: 50 us -> 48.8 us
    pallas_call x1, Pallas kernels: 48.7 us -> 47.5 us  [fused(): pl.pallas_call(functools.partial(kernel, n_ep, n_tp, cap), out_shape=[plt...]
where the time goes in v3:
time: 49.8 us; the launch traced here: 49.6 us
  Pallas kernels  48.8 us (98%)
  between operations  0.81 us (2%)
    pallas_call x1, Pallas kernels, fused(): pl.pallas_call(functools.partial(kernel, n_ep, n_tp, cap), out_shape=[plt...  47.5 us
    pallas_call x1, Pallas kernels, fused(): pl.pallas_call(flush, out_shape=[jax.ShapeDtypeStruct(shape, dtype) for s...  1.28 us

profile of v3, /device:TPU:0, one launch (start us, length us, event | category | flops | bytes accessed | tf_op | source)
XLA Modules:
  0.0 49.6 jit_solution(5416710634535470329)
XLA Ops:
  0.6 47.5 %shard_map.142 = (bf16[128,512]{1,0:T(8,128)(2,1)S(1)}, f32[2,128]{1,0:T(2,128)S(1)}, f32[8,256]{1,0:T(8,128)S(1)}, bf16[2048,128]{1,0:T(8,128)(2,1)S(1)}, bf16[...) custom-call(bf16[128,2048]{1,0:T(8,128)(2,1)} %tok_hbm.1, ...), custom_call_target="tpu_custom_call" | custom-call | tf_op jit(solution)/shard_map/pallas_call | solution.py:741
  48.2 1.3 %shard_map.143 = (bf16[128,512]{1,0:T(8,128)(2,1)}, f32[2,128]{1,0:T(2,128)}, f32[8,256]{1,0:T(8,128)}, bf16[2048,128]{1,0:T(8,128)(2,1)}, bf16[2048,128]{1,0:T(...) custom-call(bf16[128,512]{1,0:T(8,128)(2,1)S(1)} %get-tuple-element.27.refs_0_, ...), custom_call_target="tpu_custom_call" | custom-call | tf_op jit(solution)/shard_map/pallas_call | solution.py:794

commit v4 on v3

--- a/solution.py
+++ b/solution.py
@@ -453,10 +453,11 @@
         for h in ((0, 1) if s else (1, 0)):
             src = ep_of(planes[s], h)
             send(("xs", s, h), xs.at[src], xr.at[src], BACK, tp=p_x)
-        landed(("pc", s, 0), pc.at[0, pair])
 
     def to_home(s, h):
         other = ep_of(planes[s], h)
+        if h == (0 if s else 1):
+            landed(("pc", s, 0), pc.at[0, pl.ds(planes[s] * 2, 2)])
         landed(("xs", s, h), xr.at[other])
         fin[other] = (part[p, other].astype(F32) + pc[0, other].astype(F32)
                       + xr[other].astype(F32)).astype(BF16)
@@ -782,7 +783,7 @@
             pltpu.VMEM((n_ep, n_exp, span), F32),
             pltpu.SemaphoreType.DMA((11,)),
             pltpu.SemaphoreType.DMA((SMALL + 1,)),
-            pltpu.SemaphoreType.DMA((80,)),
+            pltpu.SemaphoreType.DMA((74,)),
             pltpu.SemaphoreType.REGULAR,
         ],
         compiler_params=pltpu.CompilerParams(

time: 49.8 us -> 49.7 us (level)
  no operation moved by 1% of the time
where the time goes in v4:
time: 49.7 us; the launch traced here: 49.6 us
  Pallas kernels  48.8 us (98%)
  between operations  0.81 us (2%)
    pallas_call x1, Pallas kernels, fused(): pl.pallas_call(functools.partial(kernel, n_ep, n_tp, cap), out_shape=[plt...  47.5 us
    pallas_call x1, Pallas kernels, fused(): pl.pallas_call(flush, out_shape=[jax.ShapeDtypeStruct(shape, dtype) for s...  1.28 us

profile of v4, /device:TPU:0, one launch (start us, length us, event | category | flops | bytes accessed | tf_op | source)
XLA Modules:
  0.0 49.6 jit_solution(11745087752297278794)
XLA Ops:
  0.6 47.5 %shard_map.142 = (bf16[128,512]{1,0:T(8,128)(2,1)S(1)}, f32[2,128]{1,0:T(2,128)S(1)}, f32[8,256]{1,0:T(8,128)S(1)}, bf16[2048,128]{1,0:T(8,128)(2,1)S(1)}, bf16[...) custom-call(bf16[128,2048]{1,0:T(8,128)(2,1)} %tok_hbm.1, ...), custom_call_target="tpu_custom_call" | custom-call | tf_op jit(solution)/shard_map/pallas_call | solution.py:742
  48.1 1.3 %shard_map.143 = (bf16[128,512]{1,0:T(8,128)(2,1)}, f32[2,128]{1,0:T(2,128)}, f32[8,256]{1,0:T(8,128)}, bf16[2048,128]{1,0:T(8,128)(2,1)}, bf16[2048,128]{1,0:T(...) custom-call(bf16[128,512]{1,0:T(8,128)(2,1)S(1)} %get-tuple-element.27.refs_0_, ...), custom_call_target="tpu_custom_call" | custom-call | tf_op jit(solution)/shard_map/pallas_call | solution.py:795
